TPU v7x, 32 devices: a whole 2x2x4 slice. The times are simulated.
32 devices in a mesh: ep: 8 (over z, x), tp: 4 (over y, core).
Axes of the slice: x: 2, y: 2, z: 4, core: 2. Of those that a mesh axis runs over, the one named last changes fastest.
Arguments:
- conv_value: bfloat16 [1024, 4096], P('tp', 'ep'), may hold values from -6 to 6
- conv_gate: bfloat16 [1024, 4096], P('tp', 'ep'), may hold values from -8 to 8
- conv_kernel: bfloat16 [31, 1024], P(None, 'tp'), may hold values from -1 to 1
- norm_gain: float32 [1024], replicated, may hold values from 0.1 to 1.9
- norm_shift: float32 [1024], replicated, may hold values from -3 to 3
- out_weight: bfloat16 [1024, 4096], P(None, 'tp'), may hold values from -0.1875 to 0.1875
- expert_input: bfloat16 [1024, 4096], P('ep'), may hold values from -6 to 6
- expert_ids: int32 [1024, 2], P('ep'), may hold values from 0 to 7, as said below
- pair_logits: float32 [1024, 2], P('ep'), may hold values from -6 to 6
- group_prob: float32 [1024], P('ep'), may hold values from 0.3 to 1
- expert_gate: bfloat16 [8, 4096, 2048], P('ep', None, 'tp'), may hold values from -0.09375 to 0.09375
- expert_up: bfloat16 [8, 4096, 2048], P('ep', None, 'tp'), may hold values from -0.09375 to 0.09375
- expert_down: bfloat16 [8, 2048, 4096], P('ep', None, 'tp'), may hold values from -0.125 to 0.125
Outputs:
- mixer_out: bfloat16 [4096, 4096], P('ep', 'tp')
- expert_out: bfloat16 [1024, 4096], P('ep', 'tp')
Inputs may be any that keep to these rules, and one draw needn't show every extreme that they name: `expert_ids`: the two experts of a token differ and lie in one group, ids g * 2 to (g + 1) * 2 - 1 for some g. The 128 tokens of one index of ep name every expert exactly 32 times.
All inputs are finite; a program needn't handle non-finite values.
Results may differ from a plain program's by a relative error of at most 0.0064.
Values may be sent and summed in bfloat16 or wider, within the bound.
No kernel may reach another device: no remote copies, remote signals or barrier semaphores. Data moves between devices by JAX's collectives and lax.ppermute only.
A program may use at most 64 MiB of HBM per device.

v0:
```python
import jax
import jax.numpy as jnp
from jax import lax
from jax.experimental import pallas as pl
from jax.experimental.pallas import tpu as pltpu
from jax.sharding import PartitionSpec as P


def extended(cells, sides, width):
    for axis, dim in sides:
        count = lax.axis_size(axis)
        ends = count - 1
        head = lax.slice_in_dim(cells, 0, width, axis=dim)
        tail = lax.slice_in_dim(cells, cells.shape[dim] - width, cells.shape[dim], axis=dim)
        cells = jnp.concatenate(
            [
                lax.ppermute(tail, axis, [(i, (i + 1) % count) for i in range(ends)]),
                cells,
                lax.ppermute(head, axis, [((i + 1) % count, i) for i in range(ends)]),
            ],
            axis=dim,
        )
    return cells


def norm_swish(conv_out, norm_gain, norm_shift):
    values = conv_out.astype(jnp.float32)
    center = jnp.mean(values, axis=0, keepdims=True)
    spread = jnp.mean(jnp.square(values - center), axis=0, keepdims=True)
    normed = (values - center) * lax.rsqrt(spread + 1e-05) * norm_gain[:, None] + norm_shift[
        :, None
    ]
    return jax.nn.silu(normed).astype(jnp.bfloat16)


def route_weights(pair_logits, group_prob):
    share = jax.nn.sigmoid(pair_logits[:, 0] - pair_logits[:, 1])
    return jnp.stack([share, 1.0 - share], axis=1) * group_prob[:, None]


def local(
    conv_value,
    conv_gate,
    conv_kernel,
    norm_gain,
    norm_shift,
    out_weight,
    expert_input,
    expert_ids,
    pair_logits,
    group_prob,
    expert_gate,
    expert_up,
    expert_down,
):
    gated = (conv_value.astype(jnp.float32) * jax.nn.sigmoid(conv_gate.astype(jnp.float32))).astype(
        jnp.bfloat16
    )
    taps = conv_kernel.shape[0]
    reach = (taps - 1) // 2
    length = gated.shape[1]
    padded = extended(gated, (("ep", 1),), reach).astype(jnp.float32)
    kernel_f = conv_kernel.astype(jnp.float32)
    summed = jnp.zeros(gated.shape, jnp.float32)
    for offset in range(taps):
        summed = summed + kernel_f[offset][:, None] * padded[:, offset : offset + length]
    conv_out = summed.astype(jnp.bfloat16)
    experts = lax.axis_size("ep")
    flat = expert_ids.reshape(-1)
    onehot = (flat[:, None] == jnp.arange(experts, dtype=jnp.int32)[None, :]).astype(jnp.int32)
    before = jnp.cumsum(onehot, axis=0) - onehot
    slots = flat.shape[0] // experts
    position = flat * slots + jnp.sum(before * onehot, axis=1)
    source_row = (
        jnp.zeros_like(flat).at[position].set(jnp.arange(flat.shape[0], dtype=jnp.int32) // 2)
    )
    slice_width = expert_input.shape[1] // lax.axis_size("tp")
    columns = lax.dynamic_slice_in_dim(
        expert_input, lax.axis_index("tp") * slice_width, slice_width, 1
    )
    sliced = lax.all_to_all(columns[source_row], "ep", split_axis=0, concat_axis=0, tiled=True)
    arrived = lax.all_gather(sliced, "tp", axis=1, tiled=True)
    gate_val = jnp.dot(arrived, expert_gate[0], preferred_element_type=jnp.float32)
    up_val = jnp.dot(arrived, expert_up[0], preferred_element_type=jnp.float32)
    hidden = (jax.nn.silu(gate_val) * up_val).astype(jnp.bfloat16)
    down_local = expert_down[0]
    whole_conv = lax.all_gather(conv_out, "tp", axis=0, tiled=True)
    produced = jnp.dot(
        lax.all_gather(hidden, "tp", axis=1, tiled=True),
        down_local,
        preferred_element_type=jnp.float32,
    )
    returned = lax.all_to_all(
        produced.astype(jnp.bfloat16), "ep", split_axis=0, concat_axis=0, tiled=True
    )
    copies = returned[position].reshape(-1, 2, returned.shape[1]).astype(jnp.float32)
    weights = route_weights(pair_logits, group_prob)
    expert_out = jnp.sum(copies * weights[:, :, None], axis=1).astype(jnp.bfloat16)
    swished = norm_swish(whole_conv, norm_gain, norm_shift)
    mixer_out = lax.dot_general(
        swished, out_weight, (((0,), (0,)), ((), ())), preferred_element_type=jnp.float32
    ).astype(jnp.bfloat16)
    return (mixer_out, expert_out)


GROUPS = 4


def swapped(cells, axis, step):
    return lax.ppermute(cells, axis, [(i, i ^ step) for i in range(lax.axis_size(axis))])


def shifted(cells, team, step):
    count = lax.axis_size("ep")
    return lax.ppermute(cells, "ep", [(i, (i + step * team) % count) for i in range(count)])


def in_order(mine, other, first, axis):
    low = jnp.where(first, mine, other)
    high = jnp.where(first, other, mine)
    return jnp.concatenate([low, high], axis=axis)


def thirds(values):
    parts = []
    for _ in range(3):
        part = values.astype(jnp.bfloat16).astype(jnp.float32)
        parts.append(part)
        values = values - part
    return parts


def route_body(team, numbers, ids, logits, prob, cells, *outs):
    blocks, pick_out = outs[:-1], outs[-1]
    tokens, half = cells.shape
    share = tokens // GROUPS
    first = ids[:, 0:1]
    group = first // team - numbers[1]
    group = jnp.where(group < 0, group + GROUPS, group)
    down = lax.broadcasted_iota(jnp.int32, (tokens, tokens), 0)
    right = lax.broadcasted_iota(jnp.int32, (tokens, tokens), 1)
    group_row = jnp.sum(jnp.where(down == right, group, 0), axis=0, keepdims=True)
    ahead = jnp.where((group == group_row) & (right < down), 1, 0)
    position = group * share + jnp.sum(ahead, axis=1, keepdims=True)
    position_row = jnp.sum(jnp.where(down == right, position, 0), axis=0, keepdims=True)
    pick = jnp.where(position_row == down, 1.0, 0.0).astype(jnp.bfloat16)
    pick_out[...] = pick
    share_0 = jax.nn.sigmoid(logits[:, 0:1] - logits[:, 1:2])
    weight_0 = share_0 * prob[...]
    weight_1 = (1.0 - share_0) * prob[...]
    straight = first - (first // team) * team == 0
    parts = thirds(jnp.where(straight, weight_0, weight_1)) + thirds(
        jnp.where(straight, weight_1, weight_0)
    )
    lane = lax.broadcasted_iota(jnp.int32, (tokens, 128), 1)
    extra = jnp.zeros((tokens, 128), jnp.float32)
    for at, part in enumerate(parts):
        extra = jnp.where(lane == at, part, extra)
    moved = jnp.dot(pick, cells[...], preferred_element_type=jnp.float32).astype(jnp.bfloat16)
    carried = jnp.dot(
        pick, extra.astype(jnp.bfloat16), preferred_element_type=jnp.float32
    ).astype(jnp.bfloat16)
    for at, block in enumerate(blocks):
        block[:, :half] = moved[at * share : (at + 1) * share]
        block[:, half:] = carried[at * share : (at + 1) * share]


def route(numbers, expert_ids, pair_logits, group_prob, expert_input, team):
    tokens, width = expert_input.shape
    half = width // 2
    share = tokens // GROUPS

    def whole(shape):
        return pl.BlockSpec(shape, lambda i, n: (0, 0))

    block = (share, half + 128)
    return pl.pallas_call(
        lambda *refs: route_body(team, *refs),
        grid_spec=pltpu.PrefetchScalarGridSpec(
            num_scalar_prefetch=1,
            grid=(1,),
            in_specs=[
                whole((tokens, 2)),
                whole((tokens, 2)),
                whole((tokens, 1)),
                pl.BlockSpec((tokens, half), lambda i, n: (0, n[0])),
            ],
            out_specs=[whole(block)] * GROUPS + [whole((tokens, tokens))],
        ),
        out_shape=[jax.ShapeDtypeStruct(block, jnp.bfloat16)] * GROUPS
        + [jax.ShapeDtypeStruct((tokens, tokens), jnp.bfloat16)],
    )(numbers, expert_ids, pair_logits, group_prob[:, None], expert_input)


def paired(
    conv_value,
    conv_gate,
    conv_kernel,
    norm_gain,
    norm_shift,
    out_weight,
    expert_input,
    expert_ids,
    pair_logits,
    group_prob,
    expert_gate,
    expert_up,
    expert_down,
):
    team = lax.axis_size("ep") // GROUPS
    tokens = expert_input.shape[0]
    share = tokens // GROUPS
    half = expert_input.shape[1] // 2
    place = lax.axis_index("ep")
    own_first = place % team == 0
    spot = lax.axis_index("tp")
    core_first = spot % 2 == 0
    chip_first = spot // 2 == 0

    gated = (conv_value.astype(jnp.float32) * jax.nn.sigmoid(conv_gate.astype(jnp.float32))).astype(
        jnp.bfloat16
    )
    taps = conv_kernel.shape[0]
    reach = (taps - 1) // 2
    length = gated.shape[1]
    padded = extended(gated, (("ep", 1),), reach)

    numbers = jnp.stack([spot % 2, place // team]).astype(jnp.int32)
    *sent, pick = route(numbers, expert_ids, pair_logits, group_prob, expert_input, team)
    padded, sent = lax.optimization_barrier((padded, sent))
    blocks = [sent[0]]
    for step in range(1, GROUPS):
        blocks.append(shifted(sent[step], team, step))
    across = []
    for block in blocks:
        across.append(swapped(block[:, :half], "ep", 1))
    came = jnp.concatenate(blocks, axis=0)

    padded = padded.astype(jnp.float32)
    kernel_f = conv_kernel.astype(jnp.float32)
    summed = jnp.zeros(gated.shape, jnp.float32)
    for offset in range(taps):
        summed = summed + kernel_f[offset][:, None] * padded[:, offset : offset + length]
    conv_out = summed.astype(jnp.bfloat16)
    conv_out = lax.optimization_barrier(conv_out)

    def gathered(cells, axis):
        far = swapped(cells, "tp", 2)
        near = swapped(cells, "tp", 1)
        both = swapped(far, "tp", 1)
        same_chip = in_order(cells, near, core_first, axis)
        other_chip = in_order(far, both, core_first, axis)
        return in_order(same_chip, other_chip, chip_first, axis)

    swished = norm_swish(gathered(conv_out, 0), norm_gain, norm_shift)
    mixer_out = lax.dot_general(
        swished, out_weight, (((0,), (0,)), ((), ())), preferred_element_type=jnp.float32
    ).astype(jnp.bfloat16)

    def hidden_of(mine):
        rows = in_order(mine, swapped(mine, "tp", 1), core_first, 1)
        gate_val = jnp.dot(rows, expert_gate[0], preferred_element_type=jnp.float32)
        up_val = jnp.dot(rows, expert_up[0], preferred_element_type=jnp.float32)
        hidden = (jax.nn.silu(gate_val) * up_val).astype(jnp.bfloat16)
        return gathered(lax.optimization_barrier(hidden), 1)

    hidden_a = hidden_of(came[:, :half])
    hidden_b = hidden_of(jnp.concatenate(across, axis=0))
    produced_b = jnp.dot(hidden_b, expert_down[0], preferred_element_type=jnp.float32).astype(
        jnp.bfloat16
    )
    produced_a = jnp.dot(hidden_a, expert_down[0], preferred_element_type=jnp.float32).astype(
        jnp.bfloat16
    )
    carried = came[:, half:].astype(jnp.float32)
    for_low = carried[:, 0:1] + carried[:, 1:2] + carried[:, 2:3]
    for_high = carried[:, 3:4] + carried[:, 4:5] + carried[:, 5:6]
    weight_mine = jnp.where(own_first, for_low, for_high)
    weight_other = jnp.where(own_first, for_high, for_low)

    def joined(low, high):
        given = swapped(produced_b[low:high], "ep", 1)
        return (
            produced_a[low:high].astype(jnp.float32) * weight_mine[low:high]
            + given.astype(jnp.float32) * weight_other[low:high]
        ).astype(jnp.bfloat16)

    early = joined(share, 3 * share)
    back = [shifted(early[:share], team, -1), shifted(early[share:], team, -2)]
    last = joined(3 * share, 4 * share)
    back.append(shifted(last, team, -3))
    back.insert(0, joined(0, share))
    expert_out = lax.dot_general(
        pick,
        jnp.concatenate(back, axis=0),
        (((0,), (0,)), ((), ())),
        preferred_element_type=jnp.float32,
    ).astype(jnp.bfloat16)
    return (mixer_out, expert_out)


def solution(mesh):
    plan = paired if mesh.shape["ep"] == 2 * GROUPS and mesh.shape["tp"] == 4 else local
    placed = (
        P("tp", "ep"),
        P("tp", "ep"),
        P(None, "tp"),
        P(),
        P(),
        P(None, "tp"),
        P("ep", None),
        P("ep", None),
        P("ep", None),
        P("ep"),
        P("ep", None, "tp"),
        P("ep", None, "tp"),
        P("ep", None, "tp"),
    )
    return jax.shard_map(
        plan, mesh=mesh, in_specs=placed, out_specs=(P("ep", "tp"), P("ep", "tp")), check_vma=False
    )
```

profile of v0, /device:TPU:0, one launch (start us, length us, event | category | flops | bytes accessed | tf_op | source)
XLA Modules:
  0.0 92.1 jit_solution(17270508192824367757)
XLA Ops:
  0.6 1.3 %multiply_convert_fusion = bf16[256,512]{1,0:T(8,128)(2,1)S(1)} fusion(bf16[256,512]{1,0:T(8,128)(2,1)} %param.14, bf16[256,512]{1,0:T(8,128)(2,1)} %param.13), kind=kLoop, calls=%fused_computation.107 | loop fusion | flops 917504 | bytes 786432 | tf_op jit(solution)/shard_map/convert_element_type | solution.py:220
  2.0 0.1 fusion.93
  2.1 4.9 %collective-permute-start = (bf16[256,15]{1,0:T(8,128)(2,1)S(1)}, bf16[256,15]{1,0:T(8,128)(2,1)S(1)}, u32[]{:S(2)}, u32[]{:S(2)}) collective-permute-start(bf16[256,15]{1,0:T(8,128)(2,1)S(1)} %get-tuple-element.52), channel_id=1, source_target_pairs={{0,4},{4,8},{8,12},{12,16},{16,20},{20,24},{24,28},{1,5},{5,9},{9,... | collective-permute-start | bytes 23048 | tf_op jit(solution)/shard_map/ppermute | solution.py:17
  6.9 1.3 %collective-permute-start.1 = (bf16[256,15]{1,0:T(8,128)(2,1)S(1)}, bf16[256,15]{1,0:T(8,128)(2,1)S(1)}, u32[]{:S(2)}, u32[]{:S(2)}) collective-permute-start(bf16[256,15]{1,0:T(8,128)(2,1)S(1)} %get-tuple-element.53), channel_id=1, source_target_pairs={{4,0},{8,4},{12,8},{16,12},{20,16},{24,20},{28,24},{5,1},{9,5},{13... | collective-permute-start | bytes 23048 | tf_op jit(solution)/shard_map/ppermute | solution.py:19
  8.3 1.0 %fusion.95 = (f32[1,256]{1,0:T(1,128)S(1)}, f32[1,256]{1,0:T(1,128)S(1)}, f32[1,256]{1,0:T(1,128)S(1)}, f32[1,256]{1,0:T(1,128)S(1)}, f32[1,256]{1,0:T(1,128)S(1...) fusion(bf16[31,256]{1,0:T(8,128)(2,1)} %param.15), kind=kLoop, calls=%fused_computation.183 | loop fusion | bytes 38912 | tf_op jit(solution)/shard_map/slice | solution.py:243
  9.3 1.0 %fusion.96 = (f32[1,256]{1,0:T(1,128)S(1)}, f32[1,256]{1,0:T(1,128)S(1)}, f32[1,256]{1,0:T(1,128)S(1)}, f32[1,256]{1,0:T(1,128)S(1)}, f32[1,256]{1,0:T(1,128)S(1...) fusion(bf16[31,256]{1,0:T(8,128)(2,1)} %param.15), kind=kLoop, calls=%fused_computation.184 | loop fusion | bytes 24576 | tf_op jit(solution)/shard_map/slice | solution.py:243
  10.3 0.6 pad_add_fusion.refs_0_
  10.9 1.4 %copy.18.refs_1_ = s32[128,2]{1,0:T(8,128)} copy(s32[128,2]{0,1:T(2,128)} %param.20) | data formatting | bytes 2048 | tf_op args[7]
  12.3 1.4 %copy.19.refs_2_ = f32[128,2]{1,0:T(8,128)} copy(f32[128,2]{0,1:T(2,128)} %param.21) | data formatting | bytes 2048 | tf_op args[8]
  13.7 1.4 %copy.20.refs_3_ = f32[128,1]{1,0:T(8,128)} copy(f32[128,1]{0,1:T(1,128)} %bitcast.90) | data formatting | bytes 1024 | tf_op jit(solution)/shard_map/broadcast_in_dim | solution.py:192
  15.1 3.2 %shard_map.140 = (bf16[32,2176]{1,0:T(8,128)(2,1)}, bf16[32,2176]{1,0:T(8,128)(2,1)}, bf16[32,2176]{1,0:T(8,128)(2,1)}, bf16[32,2176]{1,0:T(8,128)(2,1)}, bf16[128,128]{1,0:T(8,128)(2,1)}) custom-call(s32[2]{0:T(128)} %pad_add_fusion.refs_0_, s32[128,2]{1,0:T(8,128)} %copy.18.refs_1_, f32[128,2]{1,0:T(8,128)} %copy.19.refs_2_, f32[128,1]{1,0:T(8,128)} %copy.20.refs_3_, ...), custom_call_target="tpu_custom_call" | custom-call | tf_op jit(solution)/shard_map/pallas_call | solution.py:177
  18.3 0.2 pad_maximum_fusion.9
  18.5 0.9 slice.344
  19.4 2.7 %collective-permute-start.12 = (bf16[32,2048]{1,0:T(8,128)(2,1)S(1)}, bf16[32,2048]{1,0:T(8,128)(2,1)S(1)}, u32[]{:S(2)}, u32[]{:S(2)}) collective-permute-start(bf16[32,2048]{1,0:T(8,128)(2,1)S(1)} %slice.344), channel_id=1, source_target_pairs={{0,4},{4,0},{8,12},{12,8},{16,20},{20,16},{24,28},{28,24},{1,5},{5... | collective-permute-start | bytes 393224 | tf_op jit(solution)/shard_map/ppermute | solution.py:110
  22.2 5.9 %fusion.36 = bf16[256,512]{1,0:T(8,128)(2,1)S(1)} fusion(f32[256,542]{1,0:T(8,128)S(1)} %convert_element_type.76, f32[256]{0:T(256)S(1)} %bitcast.89, f32[256]{0:T(256)S(1)} %bitcast.88, f32[256]{0:T(256)S(1)} %bitcast.87, f32[256]{0:T(256)S(1)} %bitcast.86, f32[256]{0:T(256)S(1)} %bitcast.85, f32[256]{0:T(256)S(1)} %bitcast.84, f32[256]{0:T(256)S(1)} %bitcast.83, ...), kind=kLoop, calls=%fused_computation.39 | loop fusion | flops 8126464 | bytes 16546816 | tf_op jit(solution)/shard_map/convert_element_type | solution.py:244
  28.2 1.6 %collective-permute-start.3 = (bf16[256,512]{1,0:T(8,128)(2,1)S(1)}, bf16[256,512]{1,0:T(8,128)(2,1)S(1)}, u32[]{:S(2)}, u32[]{:S(2)}) collective-permute-start(bf16[256,512]{1,0:T(8,128)(2,1)S(1)} %fusion.36), channel_id=1, source_target_pairs={{0,2},{1,3},{2,0},{3,1},{4,6},{5,7},{6,4},{7,5},{8,10},{9,11},{10,... | collective-permute-start | bytes 786440 | tf_op jit(solution)/shard_map/ppermute | solution.py:110
  29.8 1.6 %collective-permute-start.5 = (bf16[32,2176]{1,0:T(8,128)(2,1)S(1)}, bf16[32,2176]{1,0:T(8,128)(2,1)S(1)}, u32[]{:S(2)}, u32[]{:S(2)}) collective-permute-start(bf16[32,2176]{1,0:T(8,128)(2,1)S(1)} %copy-done.7), channel_id=1, source_target_pairs={{0,8},{4,12},{8,16},{12,20},{16,24},{20,28},{24,0},{28,4},{1,9},{5... | collective-permute-start | bytes 417800 | tf_op jit(solution)/shard_map/ppermute | solution.py:115
  31.4 2.6 %collective-permute-start.6 = (bf16[32,2176]{1,0:T(8,128)(2,1)S(1)}, bf16[32,2176]{1,0:T(8,128)(2,1)S(1)}, u32[]{:S(2)}, u32[]{:S(2)}) collective-permute-start(bf16[32,2176]{1,0:T(8,128)(2,1)S(1)} %copy-done.6), channel_id=1, source_target_pairs={{0,16},{4,20},{8,24},{12,28},{16,0},{20,4},{24,8},{28,12},{1,17},{... | collective-permute-start | bytes 417800 | tf_op jit(solution)/shard_map/ppermute | solution.py:115
  34.0 1.3 %collective-permute-start.7 = (bf16[32,2176]{1,0:T(8,128)(2,1)S(1)}, bf16[32,2176]{1,0:T(8,128)(2,1)S(1)}, u32[]{:S(2)}, u32[]{:S(2)}) collective-permute-start(bf16[32,2176]{1,0:T(8,128)(2,1)S(1)} %copy-done.5), channel_id=1, source_target_pairs={{0,24},{4,28},{8,0},{12,4},{16,8},{20,12},{24,16},{28,20},{1,25},{... | collective-permute-start | bytes 417800 | tf_op jit(solution)/shard_map/ppermute | solution.py:115
  35.4 2.9 %collective-permute-done.5 = bf16[32,2176]{1,0:T(8,128)(2,1)S(1)} collective-permute-done((bf16[32,2176]{1,0:T(8,128)(2,1)S(1)}, bf16[32,2176]{1,0:T(8,128)(2,1)S(1)}, u32[]{:S(2)}, u32[]{:S(2)}) %collective-permute-start.5) | collective-permute-done | bytes 139296 | tf_op jit(solution)/shard_map/ppermute | solution.py:115
  38.3 5.2 %collective-permute-done.6 = bf16[32,2176]{1,0:T(8,128)(2,1)S(1)} collective-permute-done((bf16[32,2176]{1,0:T(8,128)(2,1)S(1)}, bf16[32,2176]{1,0:T(8,128)(2,1)S(1)}, u32[]{:S(2)}, u32[]{:S(2)}) %collective-permute-start.6) | collective-permute-done | bytes 139296 | tf_op jit(solution)/shard_map/ppermute | solution.py:115
  43.7 1.5 %collective-permute-start.13 = (bf16[32,2048]{1,0:T(8,128)(2,1)S(1)}, bf16[32,2048]{1,0:T(8,128)(2,1)S(1)}, u32[]{:S(2)}, u32[]{:S(2)}) collective-permute-start(bf16[32,2048]{1,0:T(8,128)(2,1)S(1)} %slice.434), channel_id=1, source_target_pairs={{0,4},{4,0},{8,12},{12,8},{16,20},{20,16},{24,28},{28,24},{1,5},{5... | collective-permute-start | bytes 393224 | tf_op jit(solution)/shard_map/ppermute | solution.py:110
  45.2 0.7 collective-permute-start.14
  45.9 0.1 broadcast_select_fusion.23
  46.0 0.1 slice_reduce_fusion.4
  46.2 0.1 slice_reduce_fusion
  46.3 1.5 %collective-permute-start.15 = (bf16[32,2048]{1,0:T(8,128)(2,1)S(1)}, bf16[32,2048]{1,0:T(8,128)(2,1)S(1)}, u32[]{:S(2)}, u32[]{:S(2)}) collective-permute-start(bf16[32,2048]{1,0:T(8,128)(2,1)S(1)} %slice.436), channel_id=1, source_target_pairs={{0,4},{4,0},{8,12},{12,8},{16,20},{20,16},{24,28},{28,24},{1,5},{5... | collective-permute-start | bytes 393224 | tf_op jit(solution)/shard_map/ppermute | solution.py:110
  47.9 2.3 %collective-permute-done.13 = bf16[32,2048]{1,0:T(8,128)(2,1)S(1)} collective-permute-done((bf16[32,2048]{1,0:T(8,128)(2,1)S(1)}, bf16[32,2048]{1,0:T(8,128)(2,1)S(1)}, u32[]{:S(2)}, u32[]{:S(2)}) %collective-permute-start.13) | collective-permute-done | bytes 131104 | tf_op jit(solution)/shard_map/ppermute | solution.py:110
  50.1 2.8 %collective-permute-done.14 = bf16[32,2048]{1,0:T(8,128)(2,1)S(1)} collective-permute-done((bf16[32,2048]{1,0:T(8,128)(2,1)S(1)}, bf16[32,2048]{1,0:T(8,128)(2,1)S(1)}, u32[]{:S(2)}, u32[]{:S(2)}) %collective-permute-start.14) | collective-permute-done | bytes 131104 | tf_op jit(solution)/shard_map/ppermute | solution.py:110
  52.9 2.3 %collective-permute-done.15 = bf16[32,2048]{1,0:T(8,128)(2,1)S(1)} collective-permute-done((bf16[32,2048]{1,0:T(8,128)(2,1)S(1)}, bf16[32,2048]{1,0:T(8,128)(2,1)S(1)}, u32[]{:S(2)}, u32[]{:S(2)}) %collective-permute-start.15) | collective-permute-done | bytes 131104 | tf_op jit(solution)/shard_map/ppermute | solution.py:110
  55.4 0.2 broadcast_select_fusion.5
  55.6 0.2 convert_reduce_fusion
  55.9 0.3 fusion.14
  56.2 0.1 broadcast_select_fusion.3
  56.3 1.5 %copy-done.3 = bf16[1,4096,512]{2,1,0:T(8,128)(2,1)S(1)} copy-done((bf16[1,4096,512]{2,1,0:T(8,128)(2,1)S(1)}, bf16[1,4096,512]{2,1,0:T(8,128)(2,1)}, u32[]{:S(2)}) %copy-start.3) | copy-done | bytes 4194328
  57.8 0.7 fusion.10
  58.5 1.5 %copy-done.4 = bf16[1,4096,512]{2,1,0:T(8,128)(2,1)S(1)} copy-done((bf16[1,4096,512]{2,1,0:T(8,128)(2,1)S(1)}, bf16[1,4096,512]{2,1,0:T(8,128)(2,1)}, u32[]{:S(2)}) %copy-start.4) | copy-done | bytes 4194328
  60.0 0.7 multiply_convert_fusion.2
  60.7 0.6 collective-permute-start.10
  61.3 0.2 collective-permute-start.9
  61.6 0.7 fusion.8
  62.3 0.7 multiply_convert_fusion.1
  63.1 0.4 collective-permute-start.17
  63.4 1.5 %collective-permute-start.18 = (bf16[128,512]{1,0:T(8,128)(2,1)S(1)}, bf16[128,512]{1,0:T(8,128)(2,1)S(1)}, u32[]{:S(2)}, u32[]{:S(2)}) collective-permute-start(bf16[128,512]{1,0:T(8,128)(2,1)S(1)} %multiply_convert_fusion.1), channel_id=1, source_target_pairs={{0,2},{1,3},{2,0},{3,1},{4,6},{5,7},{6,4},{7,5},{8,10},{9,11},{10,... | collective-permute-start | bytes 393224 | tf_op jit(solution)/shard_map/ppermute | solution.py:110
  64.9 2.2 %collective-permute-done.10 = bf16[128,512]{1,0:T(8,128)(2,1)S(1)} collective-permute-done((bf16[128,512]{1,0:T(8,128)(2,1)S(1)}, bf16[128,512]{1,0:T(8,128)(2,1)S(1)}, u32[]{:S(2)}, u32[]{:S(2)}) %collective-permute-start.10) | collective-permute-done | bytes 131104 | tf_op jit(solution)/shard_map/ppermute | solution.py:110
  67.2 2.3 %collective-permute-done.18 = bf16[128,512]{1,0:T(8,128)(2,1)S(1)} collective-permute-done((bf16[128,512]{1,0:T(8,128)(2,1)S(1)}, bf16[128,512]{1,0:T(8,128)(2,1)S(1)}, u32[]{:S(2)}, u32[]{:S(2)}) %collective-permute-start.18) | collective-permute-done | bytes 131104 | tf_op jit(solution)/shard_map/ppermute | solution.py:110
  69.6 1.3 %collective-permute-done.19 = bf16[128,512]{1,0:T(8,128)(2,1)S(1)} collective-permute-done((bf16[128,512]{1,0:T(8,128)(2,1)S(1)}, bf16[128,512]{1,0:T(8,128)(2,1)S(1)}, u32[]{:S(2)}, u32[]{:S(2)}) %collective-permute-start.19) | collective-permute-done | bytes 131104 | tf_op jit(solution)/shard_map/ppermute | solution.py:110
  70.9 0.2 broadcast_select_fusion.7
  71.1 0.7 fusion.26
  71.9 1.5 %collective-permute-start.21 = (bf16[64,1024]{1,0:T(8,128)(2,1)S(1)}, bf16[64,1024]{1,0:T(8,128)(2,1)S(1)}, u32[]{:S(2)}, u32[]{:S(2)}) collective-permute-start(bf16[64,1024]{1,0:T(8,128)(2,1)S(1)} %slice.441), channel_id=1, source_target_pairs={{0,4},{4,0},{8,12},{12,8},{16,20},{20,16},{24,28},{28,24},{1,5},{5... | collective-permute-start | bytes 393224 | tf_op jit(solution)/shard_map/ppermute | solution.py:110
  73.4 0.6 collective-permute-start.20
  74.0 1.4 %collective-permute-start.24 = (bf16[32,1024]{1,0:T(8,128)(2,1)S(1)}, bf16[32,1024]{1,0:T(8,128)(2,1)S(1)}, u32[]{:S(2)}, u32[]{:S(2)}) collective-permute-start(bf16[32,1024]{1,0:T(8,128)(2,1)S(1)} %get-tuple-element.43), channel_id=1, source_target_pairs={{0,4},{4,0},{8,12},{12,8},{16,20},{20,16},{24,28},{28,24},{1,5},{5... | collective-permute-start | bytes 196616 | tf_op jit(solution)/shard_map/ppermute | solution.py:110
  75.4 0.7 fusion.23
  76.2 3.5 %collective-permute-done.20 = bf16[32,1024]{1,0:T(8,128)(2,1)S(1)} collective-permute-done((bf16[32,1024]{1,0:T(8,128)(2,1)S(1)}, bf16[32,1024]{1,0:T(8,128)(2,1)S(1)}, u32[]{:S(2)}, u32[]{:S(2)}) %collective-permute-start.20) | collective-permute-done | bytes 65568 | tf_op jit(solution)/shard_map/ppermute | solution.py:110
  79.6 0.7 collective-permute-done.24
  80.3 0.1 add_convert_fusion.2
  80.4 3.5 %collective-permute-start.25 = (bf16[32,1024]{1,0:T(8,128)(2,1)S(1)}, bf16[32,1024]{1,0:T(8,128)(2,1)S(1)}, u32[]{:S(2)}, u32[]{:S(2)}) collective-permute-start(bf16[32,1024]{1,0:T(8,128)(2,1)S(1)} %get-tuple-element.41), channel_id=1, source_target_pairs={{0,8},{4,12},{8,16},{12,20},{16,24},{20,28},{24,0},{28,4},{1,9},{5... | collective-permute-start | bytes 196616 | tf_op jit(solution)/shard_map/ppermute | solution.py:115
  83.9 0.1 add_convert_fusion
  84.1 1.2 %collective-permute-start.22 = (bf16[32,1024]{1,0:T(8,128)(2,1)S(1)}, bf16[32,1024]{1,0:T(8,128)(2,1)S(1)}, u32[]{:S(2)}, u32[]{:S(2)}) collective-permute-start(bf16[32,1024]{1,0:T(8,128)(2,1)S(1)} %get-tuple-element.54), channel_id=1, source_target_pairs={{0,24},{4,28},{8,0},{12,4},{16,8},{20,12},{24,16},{28,20},{1,25},{... | collective-permute-start | bytes 196616 | tf_op jit(solution)/shard_map/ppermute | solution.py:115
  85.2 0.6 collective-permute-start.23
  85.9 2.5 %convolution_convert_fusion = bf16[512,1024]{1,0:T(8,128)(2,1)} fusion(bf16[1024,1024]{1,0:T(8,128)(2,1)S(1)} %copy-done, f32[1024]{0:T(1024)S(1)} %copy-done.9, f32[1024]{0:T(1024)S(1)} %copy-done.10, f32[512]{0:T(512)S(1)} %add_rsqrt_fusion, f32[512]{0:T(512)S(1)} %broadcast_multiply_fusion, bf16[512,512]{1,0:T(8,128)(2,1)S(1)} %get-tuple-element.31, ...), kind=kOutput, calls=%fused_computation.25 | convolution fusion | flops 1081081856 | bytes 4206592 | tf_op jit(solution)/shard_map/dot_general | solution.py:256
  88.4 0.1 collective-permute-done.22
  88.5 2.6 %collective-permute-done.23 = bf16[32,1024]{1,0:T(8,128)(2,1)S(1)} collective-permute-done((bf16[32,1024]{1,0:T(8,128)(2,1)S(1)}, bf16[32,1024]{1,0:T(8,128)(2,1)S(1)}, u32[]{:S(2)}, u32[]{:S(2)}) %collective-permute-start.23) | collective-permute-done | bytes 65568 | tf_op jit(solution)/shard_map/ppermute | solution.py:115
  91.1 1.0 %convolution_convert_fusion.1 = bf16[128,1024]{1,0:T(8,128)(2,1)} fusion(bf16[128,128]{1,0:T(8,128)(2,1)S(1)} %copy-done.8, bf16[32,1024]{1,0:T(8,128)(2,1)S(1)} %collective-permute-done.25, bf16[32,1024]{1,0:T(8,128)(2,1)S(1)} %collective-permute-done.23, bf16[32,1024]{1,0:T(8,128)(2,1)S(1)} %collective-permute-done.22, ...), kind=kOutput, calls=%fused_computation.26 | convolution fusion | flops 34734080 | bytes 557056 | tf_op jit(solution)/shard_map/dot_general | solution.py:293
  (66 shorter events, 0.9 us)
Async XLA Ops:
  0.6 85.2 %copy-start = (bf16[1024,1024]{1,0:T(8,128)(2,1)S(1)}, bf16[1024,1024]{1,0:T(8,128)(2,1)}, u32[]{:S(2)}) copy-start(bf16[1024,1024]{1,0:T(8,128)(2,1)} %param.18) | copy-start | bytes 6291460
  2.1 16.3 %collective-permute-start = (bf16[256,15]{1,0:T(8,128)(2,1)S(1)}, bf16[256,15]{1,0:T(8,128)(2,1)S(1)}, u32[]{:S(2)}, u32[]{:S(2)}) collective-permute-start(bf16[256,15]{1,0:T(8,128)(2,1)S(1)} %get-tuple-element.52), channel_id=1, source_target_pairs={{0,4},{4,8},{8,12},{12,16},{16,20},{20,24},{24,28},{1,5},{5,9},{9,... | collective-permute-start | bytes 23048 | tf_op jit(solution)/shard_map/ppermute | solution.py:17
  6.9 11.4 %collective-permute-start.1 = (bf16[256,15]{1,0:T(8,128)(2,1)S(1)}, bf16[256,15]{1,0:T(8,128)(2,1)S(1)}, u32[]{:S(2)}, u32[]{:S(2)}) collective-permute-start(bf16[256,15]{1,0:T(8,128)(2,1)S(1)} %get-tuple-element.53), channel_id=1, source_target_pairs={{4,0},{8,4},{12,8},{16,12},{20,16},{24,20},{28,24},{5,1},{9,5},{13... | collective-permute-start | bytes 23048 | tf_op jit(solution)/shard_map/ppermute | solution.py:19
  19.4 14.5 %collective-permute-start.12 = (bf16[32,2048]{1,0:T(8,128)(2,1)S(1)}, bf16[32,2048]{1,0:T(8,128)(2,1)S(1)}, u32[]{:S(2)}, u32[]{:S(2)}) collective-permute-start(bf16[32,2048]{1,0:T(8,128)(2,1)S(1)} %slice.344), channel_id=1, source_target_pairs={{0,4},{4,0},{8,12},{12,8},{16,20},{20,16},{24,28},{28,24},{1,5},{5... | collective-permute-start | bytes 393224 | tf_op jit(solution)/shard_map/ppermute | solution.py:110
  22.2 5.9 %copy-start.2 = (bf16[32,2176]{1,0:T(8,128)(2,1)S(1)}, bf16[32,2176]{1,0:T(8,128)(2,1)}, u32[]{:S(2)}) copy-start(bf16[32,2176]{1,0:T(8,128)(2,1)} %get-tuple-element.18) | copy-start | bytes 417796
  22.2 7.6 %copy-start.7 = (bf16[32,2176]{1,0:T(8,128)(2,1)S(1)}, bf16[32,2176]{1,0:T(8,128)(2,1)}, u32[]{:S(2)}) copy-start(bf16[32,2176]{1,0:T(8,128)(2,1)} %get-tuple-element.19) | copy-start | bytes 417796
  22.2 9.2 %copy-start.6 = (bf16[32,2176]{1,0:T(8,128)(2,1)S(1)}, bf16[32,2176]{1,0:T(8,128)(2,1)}, u32[]{:S(2)}) copy-start(bf16[32,2176]{1,0:T(8,128)(2,1)} %get-tuple-element.20) | copy-start | bytes 417796
  22.2 11.8 %copy-start.5 = (bf16[32,2176]{1,0:T(8,128)(2,1)S(1)}, bf16[32,2176]{1,0:T(8,128)(2,1)}, u32[]{:S(2)}) copy-start(bf16[32,2176]{1,0:T(8,128)(2,1)} %get-tuple-element.21) | copy-start | bytes 417796
  28.1 18.1 %collective-permute-start.2 = (bf16[256,512]{1,0:T(8,128)(2,1)S(1)}, bf16[256,512]{1,0:T(8,128)(2,1)S(1)}, u32[]{:S(2)}, u32[]{:S(2)}) collective-permute-start(bf16[256,512]{1,0:T(8,128)(2,1)S(1)} %fusion.36), channel_id=1, source_target_pairs={{0,1},{1,0},{2,3},{3,2},{4,5},{5,4},{6,7},{7,6},{8,9},{9,8},{10,11... | collective-permute-start | bytes 786440 | tf_op jit(solution)/shard_map/ppermute | solution.py:110
  28.2 19.6 %collective-permute-start.3 = (bf16[256,512]{1,0:T(8,128)(2,1)S(1)}, bf16[256,512]{1,0:T(8,128)(2,1)S(1)}, u32[]{:S(2)}, u32[]{:S(2)}) collective-permute-start(bf16[256,512]{1,0:T(8,128)(2,1)S(1)} %fusion.36), channel_id=1, source_target_pairs={{0,2},{1,3},{2,0},{3,1},{4,6},{5,7},{6,4},{7,5},{8,10},{9,11},{10,... | collective-permute-start | bytes 786440 | tf_op jit(solution)/shard_map/ppermute | solution.py:110
  29.8 8.4 %collective-permute-start.5 = (bf16[32,2176]{1,0:T(8,128)(2,1)S(1)}, bf16[32,2176]{1,0:T(8,128)(2,1)S(1)}, u32[]{:S(2)}, u32[]{:S(2)}) collective-permute-start(bf16[32,2176]{1,0:T(8,128)(2,1)S(1)} %copy-done.7), channel_id=1, source_target_pairs={{0,8},{4,12},{8,16},{12,20},{16,24},{20,28},{24,0},{28,4},{1,9},{5... | collective-permute-start | bytes 417800 | tf_op jit(solution)/shard_map/ppermute | solution.py:115
  31.4 12.1 %collective-permute-start.6 = (bf16[32,2176]{1,0:T(8,128)(2,1)S(1)}, bf16[32,2176]{1,0:T(8,128)(2,1)S(1)}, u32[]{:S(2)}, u32[]{:S(2)}) collective-permute-start(bf16[32,2176]{1,0:T(8,128)(2,1)S(1)} %copy-done.6), channel_id=1, source_target_pairs={{0,16},{4,20},{8,24},{12,28},{16,0},{20,4},{24,8},{28,12},{1,17},{... | collective-permute-start | bytes 417800 | tf_op jit(solution)/shard_map/ppermute | solution.py:115
  34.0 9.5 %collective-permute-start.7 = (bf16[32,2176]{1,0:T(8,128)(2,1)S(1)}, bf16[32,2176]{1,0:T(8,128)(2,1)S(1)}, u32[]{:S(2)}, u32[]{:S(2)}) collective-permute-start(bf16[32,2176]{1,0:T(8,128)(2,1)S(1)} %copy-done.5), channel_id=1, source_target_pairs={{0,24},{4,28},{8,0},{12,4},{16,8},{20,12},{24,16},{28,20},{1,25},{... | collective-permute-start | bytes 417800 | tf_op jit(solution)/shard_map/ppermute | solution.py:115
  43.6 12.6 %collective-permute-start.8 = (bf16[128,2048]{1,0:T(8,128)(2,1)S(1)}, bf16[128,2048]{1,0:T(8,128)(2,1)S(1)}, u32[]{:S(2)}, u32[]{:S(2)}) collective-permute-start(bf16[128,2048]{1,0:T(8,128)(2,1)S(1)} %slice.424), channel_id=1, source_target_pairs={{0,1},{1,0},{2,3},{3,2},{4,5},{5,4},{6,7},{7,6},{8,9},{9,8},{10,11... | collective-permute-start | bytes 1572872 | tf_op jit(solution)/shard_map/ppermute | solution.py:110
  43.7 6.4 %collective-permute-start.13 = (bf16[32,2048]{1,0:T(8,128)(2,1)S(1)}, bf16[32,2048]{1,0:T(8,128)(2,1)S(1)}, u32[]{:S(2)}, u32[]{:S(2)}) collective-permute-start(bf16[32,2048]{1,0:T(8,128)(2,1)S(1)} %slice.434), channel_id=1, source_target_pairs={{0,4},{4,0},{8,12},{12,8},{16,20},{20,16},{24,28},{28,24},{1,5},{5... | collective-permute-start | bytes 393224 | tf_op jit(solution)/shard_map/ppermute | solution.py:110
  45.2 7.7 %collective-permute-start.14 = (bf16[32,2048]{1,0:T(8,128)(2,1)S(1)}, bf16[32,2048]{1,0:T(8,128)(2,1)S(1)}, u32[]{:S(2)}, u32[]{:S(2)}) collective-permute-start(bf16[32,2048]{1,0:T(8,128)(2,1)S(1)} %slice.435), channel_id=1, source_target_pairs={{0,4},{4,0},{8,12},{12,8},{16,20},{20,16},{24,28},{28,24},{1,5},{5... | collective-permute-start | bytes 393224 | tf_op jit(solution)/shard_map/ppermute | solution.py:110
  46.3 9.0 %collective-permute-start.15 = (bf16[32,2048]{1,0:T(8,128)(2,1)S(1)}, bf16[32,2048]{1,0:T(8,128)(2,1)S(1)}, u32[]{:S(2)}, u32[]{:S(2)}) collective-permute-start(bf16[32,2048]{1,0:T(8,128)(2,1)S(1)} %slice.436), channel_id=1, source_target_pairs={{0,4},{4,0},{8,12},{12,8},{16,20},{20,16},{24,28},{28,24},{1,5},{5... | collective-permute-start | bytes 393224 | tf_op jit(solution)/shard_map/ppermute | solution.py:110
  47.8 7.6 %collective-permute-start.4 = (bf16[256,512]{1,0:T(8,128)(2,1)S(1)}, bf16[256,512]{1,0:T(8,128)(2,1)S(1)}, u32[]{:S(2)}, u32[]{:S(2)}) collective-permute-start(bf16[256,512]{1,0:T(8,128)(2,1)S(1)} %collective-permute-done.3), channel_id=1, source_target_pairs={{0,1},{1,0},{2,3},{3,2},{4,5},{5,4},{6,7},{7,6},{8,9},{9,8},{10,11... | collective-permute-start | bytes 786440 | tf_op jit(solution)/shard_map/ppermute | solution.py:110
  55.3 6.2 %collective-permute-start.16 = (bf16[128,2048]{1,0:T(8,128)(2,1)S(1)}, bf16[128,2048]{1,0:T(8,128)(2,1)S(1)}, u32[]{:S(2)}, u32[]{:S(2)}) collective-permute-start(bf16[128,2048]{1,0:T(8,128)(2,1)S(1)} %constant_dynamic-update-slice_fusion.4), channel_id=1, source_target_pairs={{0,1},{1,0},{2,3},{3,2},{4,5},{5,4},{6,7},{7,6},{8,9},{9,8},{10,11... | collective-permute-start | bytes 1572872 | tf_op jit(solution)/shard_map/ppermute | solution.py:110
  55.6 2.2 %copy-start.3 = (bf16[1,4096,512]{2,1,0:T(8,128)(2,1)S(1)}, bf16[1,4096,512]{2,1,0:T(8,128)(2,1)}, u32[]{:S(2)}) copy-start(bf16[1,4096,512]{2,1,0:T(8,128)(2,1)} %param.23) | copy-start | bytes 12582916
  57.8 2.2 %copy-start.4 = (bf16[1,4096,512]{2,1,0:T(8,128)(2,1)S(1)}, bf16[1,4096,512]{2,1,0:T(8,128)(2,1)}, u32[]{:S(2)}) copy-start(bf16[1,4096,512]{2,1,0:T(8,128)(2,1)} %param.24) | copy-start | bytes 12582916
  60.7 6.4 %collective-permute-start.10 = (bf16[128,512]{1,0:T(8,128)(2,1)S(1)}, bf16[128,512]{1,0:T(8,128)(2,1)S(1)}, u32[]{:S(2)}, u32[]{:S(2)}) collective-permute-start(bf16[128,512]{1,0:T(8,128)(2,1)S(1)} %multiply_convert_fusion.2), channel_id=1, source_target_pairs={{0,2},{1,3},{2,0},{3,1},{4,6},{5,7},{6,4},{7,5},{8,10},{9,11},{10,... | collective-permute-start | bytes 393224 | tf_op jit(solution)/shard_map/ppermute | solution.py:110
  61.3 5.8 %collective-permute-start.9 = (bf16[128,512]{1,0:T(8,128)(2,1)S(1)}, bf16[128,512]{1,0:T(8,128)(2,1)S(1)}, u32[]{:S(2)}, u32[]{:S(2)}) collective-permute-start(bf16[128,512]{1,0:T(8,128)(2,1)S(1)} %multiply_convert_fusion.2), channel_id=1, source_target_pairs={{0,1},{1,0},{2,3},{3,2},{4,5},{5,4},{6,7},{7,6},{8,9},{9,8},{10,11... | collective-permute-start | bytes 393224 | tf_op jit(solution)/shard_map/ppermute | solution.py:110
  63.1 8.1 %copy-start.1 = (bf16[1,2048,1024]{2,1,0:T(8,128)(2,1)S(1)}, bf16[1,2048,1024]{2,1,0:T(8,128)(2,1)}, u32[]{:S(2)}) copy-start(bf16[1,2048,1024]{2,1,0:T(8,128)(2,1)} %param.25) | copy-start | bytes 12582916
  63.1 6.5 %collective-permute-start.17 = (bf16[128,512]{1,0:T(8,128)(2,1)S(1)}, bf16[128,512]{1,0:T(8,128)(2,1)S(1)}, u32[]{:S(2)}, u32[]{:S(2)}) collective-permute-start(bf16[128,512]{1,0:T(8,128)(2,1)S(1)} %multiply_convert_fusion.1), channel_id=1, source_target_pairs={{0,1},{1,0},{2,3},{3,2},{4,5},{5,4},{6,7},{7,6},{8,9},{9,8},{10,11... | collective-permute-start | bytes 393224 | tf_op jit(solution)/shard_map/ppermute | solution.py:110
  63.4 6.1 %collective-permute-start.18 = (bf16[128,512]{1,0:T(8,128)(2,1)S(1)}, bf16[128,512]{1,0:T(8,128)(2,1)S(1)}, u32[]{:S(2)}, u32[]{:S(2)}) collective-permute-start(bf16[128,512]{1,0:T(8,128)(2,1)S(1)} %multiply_convert_fusion.1), channel_id=1, source_target_pairs={{0,2},{1,3},{2,0},{3,1},{4,6},{5,7},{6,4},{7,5},{8,10},{9,11},{10,... | collective-permute-start | bytes 393224 | tf_op jit(solution)/shard_map/ppermute | solution.py:110
  67.1 2.4 %collective-permute-start.11 = (bf16[128,512]{1,0:T(8,128)(2,1)S(1)}, bf16[128,512]{1,0:T(8,128)(2,1)S(1)}, u32[]{:S(2)}, u32[]{:S(2)}) collective-permute-start(bf16[128,512]{1,0:T(8,128)(2,1)S(1)} %collective-permute-done.10), channel_id=1, source_target_pairs={{0,1},{1,0},{2,3},{3,2},{4,5},{5,4},{6,7},{7,6},{8,9},{9,8},{10,11... | collective-permute-start | bytes 393224 | tf_op jit(solution)/shard_map/ppermute | solution.py:110
  69.5 1.3 %collective-permute-start.19 = (bf16[128,512]{1,0:T(8,128)(2,1)S(1)}, bf16[128,512]{1,0:T(8,128)(2,1)S(1)}, u32[]{:S(2)}, u32[]{:S(2)}) collective-permute-start(bf16[128,512]{1,0:T(8,128)(2,1)S(1)} %collective-permute-done.18), channel_id=1, source_target_pairs={{0,1},{1,0},{2,3},{3,2},{4,5},{5,4},{6,7},{7,6},{8,9},{9,8},{10,11... | collective-permute-start | bytes 393224 | tf_op jit(solution)/shard_map/ppermute | solution.py:110
  71.9 12.0 %collective-permute-start.21 = (bf16[64,1024]{1,0:T(8,128)(2,1)S(1)}, bf16[64,1024]{1,0:T(8,128)(2,1)S(1)}, u32[]{:S(2)}, u32[]{:S(2)}) collective-permute-start(bf16[64,1024]{1,0:T(8,128)(2,1)S(1)} %slice.441), channel_id=1, source_target_pairs={{0,4},{4,0},{8,12},{12,8},{16,20},{20,16},{24,28},{28,24},{1,5},{5... | collective-permute-start | bytes 393224 | tf_op jit(solution)/shard_map/ppermute | solution.py:110
  73.4 6.2 %collective-permute-start.20 = (bf16[32,1024]{1,0:T(8,128)(2,1)S(1)}, bf16[32,1024]{1,0:T(8,128)(2,1)S(1)}, u32[]{:S(2)}, u32[]{:S(2)}) collective-permute-start(bf16[32,1024]{1,0:T(8,128)(2,1)S(1)} %get-tuple-element.42), channel_id=1, source_target_pairs={{0,4},{4,0},{8,12},{12,8},{16,20},{20,16},{24,28},{28,24},{1,5},{5... | collective-permute-start | bytes 196616 | tf_op jit(solution)/shard_map/ppermute | solution.py:110
  74.0 6.3 %collective-permute-start.24 = (bf16[32,1024]{1,0:T(8,128)(2,1)S(1)}, bf16[32,1024]{1,0:T(8,128)(2,1)S(1)}, u32[]{:S(2)}, u32[]{:S(2)}) collective-permute-start(bf16[32,1024]{1,0:T(8,128)(2,1)S(1)} %get-tuple-element.43), channel_id=1, source_target_pairs={{0,4},{4,0},{8,12},{12,8},{16,20},{20,16},{24,28},{28,24},{1,5},{5... | collective-permute-start | bytes 196616 | tf_op jit(solution)/shard_map/ppermute | solution.py:110
  75.4 10.4 %copy-start.9 = (f32[1024]{0:T(1024)S(1)}, f32[1024]{0:T(1024)}, u32[]{:S(2)}) copy-start(f32[1024]{0:T(1024)} %param.17) | copy-start | bytes 12292
  75.4 10.4 %copy-start.10 = (f32[1024]{0:T(1024)S(1)}, f32[1024]{0:T(1024)}, u32[]{:S(2)}) copy-start(f32[1024]{0:T(1024)} %param.16) | copy-start | bytes 12292
  80.4 8.0 %collective-permute-start.25 = (bf16[32,1024]{1,0:T(8,128)(2,1)S(1)}, bf16[32,1024]{1,0:T(8,128)(2,1)S(1)}, u32[]{:S(2)}, u32[]{:S(2)}) collective-permute-start(bf16[32,1024]{1,0:T(8,128)(2,1)S(1)} %get-tuple-element.41), channel_id=1, source_target_pairs={{0,8},{4,12},{8,16},{12,20},{16,24},{20,28},{24,0},{28,4},{1,9},{5... | collective-permute-start | bytes 196616 | tf_op jit(solution)/shard_map/ppermute | solution.py:115
  84.1 4.4 %collective-permute-start.22 = (bf16[32,1024]{1,0:T(8,128)(2,1)S(1)}, bf16[32,1024]{1,0:T(8,128)(2,1)S(1)}, u32[]{:S(2)}, u32[]{:S(2)}) collective-permute-start(bf16[32,1024]{1,0:T(8,128)(2,1)S(1)} %get-tuple-element.54), channel_id=1, source_target_pairs={{0,24},{4,28},{8,0},{12,4},{16,8},{20,12},{24,16},{28,20},{1,25},{... | collective-permute-start | bytes 196616 | tf_op jit(solution)/shard_map/ppermute | solution.py:115
  85.2 5.9 %copy-start.8 = (bf16[128,128]{1,0:T(8,128)(2,1)S(1)}, bf16[128,128]{1,0:T(8,128)(2,1)}, u32[]{:S(2)}) copy-start(bf16[128,128]{1,0:T(8,128)(2,1)} %get-tuple-element.17) | copy-start | bytes 98308
  85.2 5.9 %collective-permute-start.23 = (bf16[32,1024]{1,0:T(8,128)(2,1)S(1)}, bf16[32,1024]{1,0:T(8,128)(2,1)S(1)}, u32[]{:S(2)}, u32[]{:S(2)}) collective-permute-start(bf16[32,1024]{1,0:T(8,128)(2,1)S(1)} %get-tuple-element.55), channel_id=1, source_target_pairs={{0,16},{4,20},{8,24},{12,28},{16,0},{20,4},{24,8},{28,12},{1,17},{... | collective-permute-start | bytes 196616 | tf_op jit(solution)/shard_map/ppermute | solution.py:115
where the time goes:
time: 92.5 us; the launch traced here: 92.1 us
  starting transfers between devices  31.3 us (34%)
  waiting for transfers between devices  28.2 us (30%)
  local copies, waits for them, and re-layouts  10.7 us (12%)
  other arithmetic  9.77 us (11%)
  matrix products  7.8 us (8%)
  Pallas kernels  3.23 us (3%)
  between operations  1.08 us (1%)
    ppermute x18, waiting for transfers between devices, swapped(): lax.ppermute(cells, axis, [(i, i ^ step) for i in range(lax.axis_size(axi...  17.3 us
    ppermute x18, starting transfers between devices, swapped(): lax.ppermute(cells, axis, [(i, i ^ step) for i in range(lax.axis_size(axi...  14.4 us
    ppermute x6, waiting for transfers between devices, shifted(): lax.ppermute(cells, 'ep', [(i, (i + step * team) % count) for i in range(...  10.8 us
    ppermute x6, starting transfers between devices, shifted(): lax.ppermute(cells, 'ep', [(i, (i + step * team) % count) for i in range(...  10.8 us
    unnamed x30, local copies, waits for them, and re-layouts  5.93 us
    convert_element_type x1, other arithmetic, paired(): conv_out = summed.astype(jnp.bfloat16)  5.87 us
    ppermute x1, starting transfers between devices, extended(): lax.ppermute(tail, axis, [(i, (i + 1) % count) for i in range(ends)])  4.87 us
    pallas_call x1, Pallas kernels, route(): pl.pallas_call(lambda *refs: route_body(team, *refs), grid_spec=pltpu.Pre...  3.23 us
  transfers between devices with their start and end apart: 26, of which 12 were waited for; matrix products, arithmetic and copies ran while one was open for 23% of the time, Pallas kernels for 4%

commit v1 on v0

--- a/solution.py
+++ b/solution.py
@@ -131,36 +131,40 @@
 
 
 def route_body(team, numbers, ids, logits, prob, cells, *outs):
-    blocks, pick_out = outs[:-1], outs[-1]
+    own, own_extra, *blocks, pick_out = outs
     tokens, half = cells.shape
     share = tokens // GROUPS
-    first = ids[:, 0:1]
-    group = first // team - numbers[1]
-    group = jnp.where(group < 0, group + GROUPS, group)
+    first = ids[0:1, :]
+    group_row = first // team - numbers[1]
+    group_row = jnp.where(group_row < 0, group_row + GROUPS, group_row)
     down = lax.broadcasted_iota(jnp.int32, (tokens, tokens), 0)
     right = lax.broadcasted_iota(jnp.int32, (tokens, tokens), 1)
-    group_row = jnp.sum(jnp.where(down == right, group, 0), axis=0, keepdims=True)
-    ahead = jnp.where((group == group_row) & (right < down), 1, 0)
-    position = group * share + jnp.sum(ahead, axis=1, keepdims=True)
-    position_row = jnp.sum(jnp.where(down == right, position, 0), axis=0, keepdims=True)
+    group = jnp.sum(jnp.where(down == right, group_row, 0), axis=1, keepdims=True)
+    ahead = jnp.where((group == group_row) & (down < right), 1, 0)
+    position_row = group_row * share + jnp.sum(ahead, axis=0, keepdims=True)
     pick = jnp.where(position_row == down, 1.0, 0.0).astype(jnp.bfloat16)
     pick_out[...] = pick
-    share_0 = jax.nn.sigmoid(logits[:, 0:1] - logits[:, 1:2])
+    share_0 = jax.nn.sigmoid(logits[0:1, :] - logits[1:2, :])
     weight_0 = share_0 * prob[...]
     weight_1 = (1.0 - share_0) * prob[...]
     straight = first - (first // team) * team == 0
     parts = thirds(jnp.where(straight, weight_0, weight_1)) + thirds(
         jnp.where(straight, weight_1, weight_0)
     )
-    lane = lax.broadcasted_iota(jnp.int32, (tokens, 128), 1)
-    extra = jnp.zeros((tokens, 128), jnp.float32)
+    line = lax.broadcasted_iota(jnp.int32, (128, tokens), 0)
+    extra = jnp.zeros((128, tokens), jnp.float32)
     for at, part in enumerate(parts):
-        extra = jnp.where(lane == at, part, extra)
+        extra = jnp.where(line == at, part, extra)
     moved = jnp.dot(pick, cells[...], preferred_element_type=jnp.float32).astype(jnp.bfloat16)
-    carried = jnp.dot(
-        pick, extra.astype(jnp.bfloat16), preferred_element_type=jnp.float32
+    carried = lax.dot_general(
+        pick,
+        extra.astype(jnp.bfloat16),
+        (((1,), (1,)), ((), ())),
+        preferred_element_type=jnp.float32,
     ).astype(jnp.bfloat16)
-    for at, block in enumerate(blocks):
+    own[...] = moved[:share]
+    own_extra[...] = carried[:share]
+    for at, block in enumerate(blocks, 1):
         block[:, :half] = moved[at * share : (at + 1) * share]
         block[:, half:] = carried[at * share : (at + 1) * share]
 
@@ -174,22 +178,22 @@
         return pl.BlockSpec(shape, lambda i, n: (0, 0))
 
     block = (share, half + 128)
+    shapes = [(share, half), (share, 128)] + [block] * (GROUPS - 1) + [(tokens, tokens)]
     return pl.pallas_call(
         lambda *refs: route_body(team, *refs),
         grid_spec=pltpu.PrefetchScalarGridSpec(
             num_scalar_prefetch=1,
             grid=(1,),
             in_specs=[
-                whole((tokens, 2)),
-                whole((tokens, 2)),
-                whole((tokens, 1)),
+                whole((2, tokens)),
+                whole((2, tokens)),
+                whole((1, tokens)),
                 pl.BlockSpec((tokens, half), lambda i, n: (0, n[0])),
             ],
-            out_specs=[whole(block)] * GROUPS + [whole((tokens, tokens))],
+            out_specs=[whole(shape) for shape in shapes],
         ),
-        out_shape=[jax.ShapeDtypeStruct(block, jnp.bfloat16)] * GROUPS
-        + [jax.ShapeDtypeStruct((tokens, tokens), jnp.bfloat16)],
-    )(numbers, expert_ids, pair_logits, group_prob[:, None], expert_input)
+        out_shape=[jax.ShapeDtypeStruct(shape, jnp.bfloat16) for shape in shapes],
+    )(numbers, expert_ids.T, pair_logits.T, group_prob[None, :], expert_input)
 
 
 def paired(
@@ -227,22 +231,27 @@
 
     numbers = jnp.stack([spot % 2, place // team]).astype(jnp.int32)
     *sent, pick = route(numbers, expert_ids, pair_logits, group_prob, expert_input, team)
-    padded, sent = lax.optimization_barrier((padded, sent))
-    blocks = [sent[0]]
-    for step in range(1, GROUPS):
-        blocks.append(shifted(sent[step], team, step))
+    padded, sent, conv_kernel = lax.optimization_barrier((padded, sent, conv_kernel))
+    own, own_extra, *sent = sent
+    arrivals = []
+    for step, block in enumerate(sent, 1):
+        arrivals.append(shifted(block, team, step))
+    blocks = [own] + [block[:, :half] for block in arrivals]
     across = []
     for block in blocks:
-        across.append(swapped(block[:, :half], "ep", 1))
-    came = jnp.concatenate(blocks, axis=0)
-
-    padded = padded.astype(jnp.float32)
+        across.append(swapped(block, "ep", 1))
+
     kernel_f = conv_kernel.astype(jnp.float32)
-    summed = jnp.zeros(gated.shape, jnp.float32)
-    for offset in range(taps):
-        summed = summed + kernel_f[offset][:, None] * padded[:, offset : offset + length]
-    conv_out = summed.astype(jnp.bfloat16)
-    conv_out = lax.optimization_barrier(conv_out)
+    tap = [kernel_f[offset][:, None] for offset in range(taps)]
+    pieces = []
+    wide = length // 2
+    for piece in range(2):
+        window = padded[:, piece * wide : (piece + 1) * wide + taps - 1].astype(jnp.float32)
+        summed = jnp.zeros((gated.shape[0], wide), jnp.float32)
+        for offset in range(taps):
+            summed = summed + tap[offset] * window[:, offset : offset + wide]
+        pieces.append(lax.optimization_barrier(summed.astype(jnp.bfloat16)))
+    conv_out = lax.optimization_barrier(jnp.concatenate(pieces, axis=1))
 
     def gathered(cells, axis):
         far = swapped(cells, "tp", 2)
@@ -264,7 +273,7 @@
         hidden = (jax.nn.silu(gate_val) * up_val).astype(jnp.bfloat16)
         return gathered(lax.optimization_barrier(hidden), 1)
 
-    hidden_a = hidden_of(came[:, :half])
+    hidden_a = hidden_of(jnp.concatenate(blocks, axis=0))
     hidden_b = hidden_of(jnp.concatenate(across, axis=0))
     produced_b = jnp.dot(hidden_b, expert_down[0], preferred_element_type=jnp.float32).astype(
         jnp.bfloat16
@@ -272,7 +281,8 @@
     produced_a = jnp.dot(hidden_a, expert_down[0], preferred_element_type=jnp.float32).astype(
         jnp.bfloat16
     )
-    carried = came[:, half:].astype(jnp.float32)
+    carried = jnp.concatenate([own_extra] + [block[:, half:] for block in arrivals], axis=0)
+    carried = carried.astype(jnp.float32)
     for_low = carried[:, 0:1] + carried[:, 1:2] + carried[:, 2:3]
     for_high = carried[:, 3:4] + carried[:, 4:5] + carried[:, 5:6]
     weight_mine = jnp.where(own_first, for_low, for_high)

time: 92.5 us -> 85.7 us (0.926)
  local copies, waits for them, and re-layouts: 10.7 us -> 3.39 us
  starting transfers between devices: 31.3 us -> 29.5 us
  other arithmetic: 9.77 us -> 11.2 us
  waiting for transfers between devices: 28.2 us -> 29.6 us
    unnamed x30 -> x29, local copies, waits for them, and re-layouts: 5.93 us -> 2.92 us
    slice x7 -> x8, local copies, waits for them, and re-layouts: 2.97 us -> 0.07 us  [the longest x2 0.03 us: paired(): tap = [kernel_f[offset][:, None] for offset in range(taps)]]
    ppermute x18, starting transfers between devices: 14.4 us -> 12.7 us  [swapped(): lax.ppermute(cells, axis, [(i, i ^ step) for i in range(lax.axis_size(axi...]
    broadcast_in_dim x1 -> x0, local copies, waits for them, and re-layouts: 1.39 us -> none  [route(): group_prob[:, None]]
    ppermute x1, waiting for transfers between devices: 0.01 us -> 1.26 us  [extended(): lax.ppermute(head, axis, [((i + 1) % count, i) for i in range(ends)])]
    ppermute x18, waiting for transfers between devices: 17.3 us -> 18.6 us  [swapped(): lax.ppermute(cells, axis, [(i, i ^ step) for i in range(lax.axis_size(axi...]
    convert_element_type x3 -> x4, other arithmetic: 5.92 us -> 7.08 us  [the longest x2 7.02 us: paired(): pieces.append(lax.optimization_barrier(summed.astype(jnp.bfloat16)))]
    ppermute x6, waiting for transfers between devices: 10.8 us -> 9.79 us  [shifted(): lax.ppermute(cells, 'ep', [(i, (i + step * team) % count) for i in range(...]
  transfers between devices with their start and end apart: 26 -> 26, of which waited for: 12 -> 13; matrix products, arithmetic and copies ran while one was open for 23% -> 19% of each run, Pallas kernels for 4% -> 3%
where the time goes in v1:
time: 85.7 us; the launch traced here: 85.4 us
  waiting for transfers between devices  29.6 us (35%)
  starting transfers between devices  29.5 us (34%)
  other arithmetic  11.2 us (13%)
  matrix products  7.8 us (9%)
  local copies, waits for them, and re-layouts  3.39 us (4%)
  Pallas kernels  2.93 us (3%)
  between operations  1.09 us (1%)
    ppermute x18, waiting for transfers between devices, swapped(): lax.ppermute(cells, axis, [(i, i ^ step) for i in range(lax.axis_size(axi...  18.6 us
    ppermute x18, starting transfers between devices, swapped(): lax.ppermute(cells, axis, [(i, i ^ step) for i in range(lax.axis_size(axi...  12.7 us
    ppermute x6, starting transfers between devices, shifted(): lax.ppermute(cells, 'ep', [(i, (i + step * team) % count) for i in range(...  10.6 us
    ppermute x6, waiting for transfers between devices, shifted(): lax.ppermute(cells, 'ep', [(i, (i + step * team) % count) for i in range(...  9.79 us
    convert_element_type x2, other arithmetic, paired(): pieces.append(lax.optimization_barrier(summed.astype(jnp.bfloat16)))  7.02 us
    ppermute x1, starting transfers between devices, extended(): lax.ppermute(tail, axis, [(i, (i + 1) % count) for i in range(ends)])  4.87 us
    pallas_call x1, Pallas kernels, route(): pl.pallas_call(lambda *refs: route_body(team, *refs), grid_spec=pltpu.Pre...  2.93 us
    unnamed x29, local copies, waits for them, and re-layouts  2.92 us
  transfers between devices with their start and end apart: 26, of which 13 were waited for; matrix products, arithmetic and copies ran while one was open for 19% of the time, Pallas kernels for 3%

profile of v1, /device:TPU:0, one launch (start us, length us, event | category | flops | bytes accessed | tf_op | source)
XLA Modules:
  0.0 85.4 jit_solution(8613595805785059881)
XLA Ops:
  0.7 1.3 %multiply_convert_fusion = bf16[256,512]{1,0:T(8,128)(2,1)S(1)} fusion(bf16[256,512]{1,0:T(8,128)(2,1)} %param.14, bf16[256,512]{1,0:T(8,128)(2,1)} %param.13), kind=kLoop, calls=%fused_computation.46 | loop fusion | flops 917504 | bytes 786432 | tf_op jit(solution)/shard_map/convert_element_type | solution.py:224
  2.0 0.1 fusion.124
  2.1 4.9 %collective-permute-start = (bf16[256,15]{1,0:T(8,128)(2,1)S(1)}, bf16[256,15]{1,0:T(8,128)(2,1)S(1)}, u32[]{:S(2)}, u32[]{:S(2)}) collective-permute-start(bf16[256,15]{1,0:T(8,128)(2,1)S(1)} %get-tuple-element.60), channel_id=1, source_target_pairs={{0,4},{4,8},{8,12},{12,16},{16,20},{20,24},{24,28},{1,5},{5,9},{9,... | collective-permute-start | bytes 23048 | tf_op jit(solution)/shard_map/ppermute | solution.py:17
  7.0 1.3 %collective-permute-start.1 = (bf16[256,15]{1,0:T(8,128)(2,1)S(1)}, bf16[256,15]{1,0:T(8,128)(2,1)S(1)}, u32[]{:S(2)}, u32[]{:S(2)}) collective-permute-start(bf16[256,15]{1,0:T(8,128)(2,1)S(1)} %get-tuple-element.61), channel_id=1, source_target_pairs={{4,0},{8,4},{12,8},{16,12},{20,16},{24,20},{28,24},{5,1},{9,5},{13... | collective-permute-start | bytes 23048 | tf_op jit(solution)/shard_map/ppermute | solution.py:19
  8.3 0.6 pad_add_fusion.refs_0_
  8.9 2.9 %shard_map.140 = (bf16[32,2048]{1,0:T(8,128)(2,1)}, bf16[32,128]{1,0:T(8,128)(2,1)}, bf16[32,2176]{1,0:T(8,128)(2,1)}, bf16[32,2176]{1,0:T(8,128)(2,1)}, bf16[32...) custom-call(s32[2]{0:T(128)} %pad_add_fusion.refs_0_, s32[2,128]{1,0:T(2,128)} %bitcast.123, f32[2,128]{1,0:T(2,128)} %bitcast.124, ...), custom_call_target="tpu_custom_call" | custom-call | tf_op jit(solution)/shard_map/pallas_call | solution.py:182
  11.9 1.3 %collective-permute-done.1 = bf16[256,15]{1,0:T(8,128)(2,1)S(1)} collective-permute-done((bf16[256,15]{1,0:T(8,128)(2,1)S(1)}, bf16[256,15]{1,0:T(8,128)(2,1)S(1)}, u32[]{:S(2)}, u32[]{:S(2)}) %collective-permute-start.1) | collective-permute-done | bytes 7712 | tf_op jit(solution)/shard_map/ppermute | solution.py:19
  13.1 0.2 pad_maximum_fusion.10
  13.4 2.5 %collective-permute-start.12 = (bf16[32,2048]{1,0:T(8,128)(2,1)}, bf16[32,2048]{1,0:T(8,128)(2,1)S(1)}, u32[]{:S(2)}, u32[]{:S(2)}) collective-permute-start(bf16[32,2048]{1,0:T(8,128)(2,1)} %get-tuple-element.23), channel_id=1, source_target_pairs={{0,4},{4,0},{8,12},{12,8},{16,20},{20,16},{24,28},{28,24},{1,5},{5... | collective-permute-start | bytes 393224 | tf_op jit(solution)/shard_map/ppermute | solution.py:110
  15.9 3.5 %fusion.73 = bf16[256,256]{1,0:T(8,128)(2,1)S(1)} fusion(f32[256,286]{1,0:T(8,128)S(1)} %get-tuple-element.46, f32[256]{0:T(256)S(1)} %bitcast.121, f32[256]{0:T(256)S(1)} %bitcast.119, f32[256]{0:T(256)S(1)} %bitcast.117, f32[256]{0:T(256)S(1)} %bitcast.115, f32[256]{0:T(256)S(1)} %bitcast.113, f32[256]{0:T(256)S(1)} %bitcast.111, f32[256]{0:T(256)S(1)} %bitcast.109, ...), kind=kLoop, calls=%fused_computation.118 | loop fusion | flops 4063232 | bytes 8289280 | tf_op jit(solution)/shard_map/convert_element_type | solution.py:253
  19.5 3.5 %fusion.42 = bf16[256,256]{1,0:T(8,128)(2,1)S(1)} fusion(f32[256,286]{1,0:T(8,128)S(1)} %get-tuple-element.47, f32[256]{0:T(256)S(1)} %bitcast.122, f32[256]{0:T(256)S(1)} %bitcast.120, f32[256]{0:T(256)S(1)} %bitcast.118, f32[256]{0:T(256)S(1)} %bitcast.116, f32[256]{0:T(256)S(1)} %bitcast.114, f32[256]{0:T(256)S(1)} %bitcast.112, f32[256]{0:T(256)S(1)} %bitcast.110, ...), kind=kLoop, calls=%fused_computation.56 | loop fusion | flops 4063232 | bytes 8289280 | tf_op jit(solution)/shard_map/convert_element_type | solution.py:253
  23.1 0.1 collective-permute-start.2
  23.1 1.6 %collective-permute-start.3 = (bf16[256,512]{1,0:T(8,128)(2,1)S(1)}, bf16[256,512]{1,0:T(8,128)(2,1)S(1)}, u32[]{:S(2)}, u32[]{:S(2)}) collective-permute-start(bf16[256,512]{1,0:T(8,128)(2,1)S(1)} %pad_maximum_fusion.12), channel_id=1, source_target_pairs={{0,2},{1,3},{2,0},{3,1},{4,6},{5,7},{6,4},{7,5},{8,10},{9,11},{10,... | collective-permute-start | bytes 786440 | tf_op jit(solution)/shard_map/ppermute | solution.py:110
  24.7 1.6 %collective-permute-start.5 = (bf16[32,2176]{1,0:T(8,128)(2,1)S(1)}, bf16[32,2176]{1,0:T(8,128)(2,1)S(1)}, u32[]{:S(2)}, u32[]{:S(2)}) collective-permute-start(bf16[32,2176]{1,0:T(8,128)(2,1)S(1)} %copy-done.9), channel_id=1, source_target_pairs={{0,8},{4,12},{8,16},{12,20},{16,24},{20,28},{24,0},{28,4},{1,9},{5... | collective-permute-start | bytes 417800 | tf_op jit(solution)/shard_map/ppermute | solution.py:115
  26.3 1.5 %collective-permute-start.6 = (bf16[32,2176]{1,0:T(8,128)(2,1)S(1)}, bf16[32,2176]{1,0:T(8,128)(2,1)S(1)}, u32[]{:S(2)}, u32[]{:S(2)}) collective-permute-start(bf16[32,2176]{1,0:T(8,128)(2,1)S(1)} %copy-done.8), channel_id=1, source_target_pairs={{0,16},{4,20},{8,24},{12,28},{16,0},{20,4},{24,8},{28,12},{1,17},{... | collective-permute-start | bytes 417800 | tf_op jit(solution)/shard_map/ppermute | solution.py:115
  27.9 2.4 %collective-permute-start.7 = (bf16[32,2176]{1,0:T(8,128)(2,1)S(1)}, bf16[32,2176]{1,0:T(8,128)(2,1)S(1)}, u32[]{:S(2)}, u32[]{:S(2)}) collective-permute-start(bf16[32,2176]{1,0:T(8,128)(2,1)S(1)} %copy-done.7), channel_id=1, source_target_pairs={{0,24},{4,28},{8,0},{12,4},{16,8},{20,12},{24,16},{28,20},{1,25},{... | collective-permute-start | bytes 417800 | tf_op jit(solution)/shard_map/ppermute | solution.py:115
  30.3 2.9 %collective-permute-done.5 = bf16[32,2176]{1,0:T(8,128)(2,1)S(1)} collective-permute-done((bf16[32,2176]{1,0:T(8,128)(2,1)S(1)}, bf16[32,2176]{1,0:T(8,128)(2,1)S(1)}, u32[]{:S(2)}, u32[]{:S(2)}) %collective-permute-start.5) | collective-permute-done | bytes 139296 | tf_op jit(solution)/shard_map/ppermute | solution.py:115
  33.2 5.1 %collective-permute-done.6 = bf16[32,2176]{1,0:T(8,128)(2,1)S(1)} collective-permute-done((bf16[32,2176]{1,0:T(8,128)(2,1)S(1)}, bf16[32,2176]{1,0:T(8,128)(2,1)S(1)}, u32[]{:S(2)}, u32[]{:S(2)}) %collective-permute-start.6) | collective-permute-done | bytes 139296 | tf_op jit(solution)/shard_map/ppermute | solution.py:115
  38.4 0.1 broadcast_select_fusion.23
  38.5 0.1 slice_reduce_fusion
  38.6 0.2 slice_reduce_fusion.4
  38.8 0.5 collective-permute-start.13
  39.3 1.7 %collective-permute-start.14 = (bf16[32,2048]{1,0:T(8,128)(2,1)S(1)}, bf16[32,2048]{1,0:T(8,128)(2,1)S(1)}, u32[]{:S(2)}, u32[]{:S(2)}) collective-permute-start(bf16[32,2048]{1,0:T(8,128)(2,1)S(1)} %slice.588), channel_id=1, source_target_pairs={{0,4},{4,0},{8,12},{12,8},{16,20},{20,16},{24,28},{28,24},{1,5},{5... | collective-permute-start | bytes 393224 | tf_op jit(solution)/shard_map/ppermute | solution.py:110
  41.0 0.5 collective-permute-start.15
  41.5 0.1 collective-permute-start.8
  41.6 0.5 collective-permute-start.4
  42.2 3.1 %collective-permute-done.13 = bf16[32,2048]{1,0:T(8,128)(2,1)S(1)} collective-permute-done((bf16[32,2048]{1,0:T(8,128)(2,1)S(1)}, bf16[32,2048]{1,0:T(8,128)(2,1)S(1)}, u32[]{:S(2)}, u32[]{:S(2)}) %collective-permute-start.13) | collective-permute-done | bytes 131104 | tf_op jit(solution)/shard_map/ppermute | solution.py:110
  45.2 2.8 %collective-permute-done.14 = bf16[32,2048]{1,0:T(8,128)(2,1)S(1)} collective-permute-done((bf16[32,2048]{1,0:T(8,128)(2,1)S(1)}, bf16[32,2048]{1,0:T(8,128)(2,1)S(1)}, u32[]{:S(2)}, u32[]{:S(2)}) %collective-permute-start.14) | collective-permute-done | bytes 131104 | tf_op jit(solution)/shard_map/ppermute | solution.py:110
  48.0 1.8 %collective-permute-done.15 = bf16[32,2048]{1,0:T(8,128)(2,1)S(1)} collective-permute-done((bf16[32,2048]{1,0:T(8,128)(2,1)S(1)}, bf16[32,2048]{1,0:T(8,128)(2,1)S(1)}, u32[]{:S(2)}, u32[]{:S(2)}) %collective-permute-start.15) | collective-permute-done | bytes 131104 | tf_op jit(solution)/shard_map/ppermute | solution.py:110
  50.0 0.2 broadcast_select_fusion.5
  50.2 0.2 convert_reduce_fusion
  50.4 0.3 fusion.14
  50.7 0.2 broadcast_select_fusion.3
  51.0 1.4 %copy-done.5 = bf16[1,4096,512]{2,1,0:T(8,128)(2,1)S(1)} copy-done((bf16[1,4096,512]{2,1,0:T(8,128)(2,1)S(1)}, bf16[1,4096,512]{2,1,0:T(8,128)(2,1)}, u32[]{:S(2)}) %copy-start.5) | copy-done | bytes 4194328
  52.3 0.7 fusion.10
  53.1 1.5 %copy-done.6 = bf16[1,4096,512]{2,1,0:T(8,128)(2,1)S(1)} copy-done((bf16[1,4096,512]{2,1,0:T(8,128)(2,1)S(1)}, bf16[1,4096,512]{2,1,0:T(8,128)(2,1)}, u32[]{:S(2)}) %copy-start.6) | copy-done | bytes 4194328
  54.5 0.7 multiply_convert_fusion.2
  55.3 0.6 collective-permute-start.10
  55.8 0.2 collective-permute-start.9
  56.0 0.1 broadcast_select_fusion.1
  56.1 0.7 fusion.8
  56.8 0.7 multiply_convert_fusion.1
  57.6 0.4 collective-permute-start.17
  58.0 1.5 %collective-permute-start.18 = (bf16[128,512]{1,0:T(8,128)(2,1)S(1)}, bf16[128,512]{1,0:T(8,128)(2,1)S(1)}, u32[]{:S(2)}, u32[]{:S(2)}) collective-permute-start(bf16[128,512]{1,0:T(8,128)(2,1)S(1)} %multiply_convert_fusion.1), channel_id=1, source_target_pairs={{0,2},{1,3},{2,0},{3,1},{4,6},{5,7},{6,4},{7,5},{8,10},{9,11},{10,... | collective-permute-start | bytes 393224 | tf_op jit(solution)/shard_map/ppermute | solution.py:110
  59.5 2.2 %collective-permute-done.10 = bf16[128,512]{1,0:T(8,128)(2,1)S(1)} collective-permute-done((bf16[128,512]{1,0:T(8,128)(2,1)S(1)}, bf16[128,512]{1,0:T(8,128)(2,1)S(1)}, u32[]{:S(2)}, u32[]{:S(2)}) %collective-permute-start.10) | collective-permute-done | bytes 131104 | tf_op jit(solution)/shard_map/ppermute | solution.py:110
  61.7 2.3 %collective-permute-done.18 = bf16[128,512]{1,0:T(8,128)(2,1)S(1)} collective-permute-done((bf16[128,512]{1,0:T(8,128)(2,1)S(1)}, bf16[128,512]{1,0:T(8,128)(2,1)S(1)}, u32[]{:S(2)}, u32[]{:S(2)}) %collective-permute-start.18) | collective-permute-done | bytes 131104 | tf_op jit(solution)/shard_map/ppermute | solution.py:110
  64.1 1.3 %collective-permute-done.19 = bf16[128,512]{1,0:T(8,128)(2,1)S(1)} collective-permute-done((bf16[128,512]{1,0:T(8,128)(2,1)S(1)}, bf16[128,512]{1,0:T(8,128)(2,1)S(1)}, u32[]{:S(2)}, u32[]{:S(2)}) %collective-permute-start.19) | collective-permute-done | bytes 131104 | tf_op jit(solution)/shard_map/ppermute | solution.py:110
  65.4 0.2 broadcast_select_fusion.7
  65.6 0.7 fusion.26
  66.4 0.5 collective-permute-start.21
  66.9 1.6 %collective-permute-start.20 = (bf16[32,1024]{1,0:T(8,128)(2,1)S(1)}, bf16[32,1024]{1,0:T(8,128)(2,1)S(1)}, u32[]{:S(2)}, u32[]{:S(2)}) collective-permute-start(bf16[32,1024]{1,0:T(8,128)(2,1)S(1)} %get-tuple-element.50), channel_id=1, source_target_pairs={{0,4},{4,0},{8,12},{12,8},{16,20},{20,16},{24,28},{28,24},{1,5},{5... | collective-permute-start | bytes 196616 | tf_op jit(solution)/shard_map/ppermute | solution.py:110
  68.5 0.4 collective-permute-start.24
  68.9 0.7 fusion.23
  69.7 4.5 %collective-permute-done.20 = bf16[32,1024]{1,0:T(8,128)(2,1)S(1)} collective-permute-done((bf16[32,1024]{1,0:T(8,128)(2,1)S(1)}, bf16[32,1024]{1,0:T(8,128)(2,1)S(1)}, u32[]{:S(2)}, u32[]{:S(2)}) %collective-permute-start.20) | collective-permute-done | bytes 65568 | tf_op jit(solution)/shard_map/ppermute | solution.py:110
  74.1 0.7 collective-permute-done.24
  74.8 0.1 add_convert_fusion.2
  74.9 3.6 %collective-permute-start.25 = (bf16[32,1024]{1,0:T(8,128)(2,1)S(1)}, bf16[32,1024]{1,0:T(8,128)(2,1)S(1)}, u32[]{:S(2)}, u32[]{:S(2)}) collective-permute-start(bf16[32,1024]{1,0:T(8,128)(2,1)S(1)} %get-tuple-element.49), channel_id=1, source_target_pairs={{0,8},{4,12},{8,16},{12,20},{16,24},{20,28},{24,0},{28,4},{1,9},{5... | collective-permute-start | bytes 196616 | tf_op jit(solution)/shard_map/ppermute | solution.py:115
  78.5 0.1 add_convert_fusion
  78.7 0.5 collective-permute-start.22
  79.2 1.0 %collective-permute-start.23 = (bf16[32,1024]{1,0:T(8,128)(2,1)S(1)}, bf16[32,1024]{1,0:T(8,128)(2,1)S(1)}, u32[]{:S(2)}, u32[]{:S(2)}) collective-permute-start(bf16[32,1024]{1,0:T(8,128)(2,1)S(1)} %get-tuple-element.63), channel_id=1, source_target_pairs={{0,16},{4,20},{8,24},{12,28},{16,0},{20,4},{24,8},{28,12},{1,17},{... | collective-permute-start | bytes 196616 | tf_op jit(solution)/shard_map/ppermute | solution.py:115
  80.2 2.5 %convolution_convert_fusion = bf16[512,1024]{1,0:T(8,128)(2,1)} fusion(bf16[1024,1024]{1,0:T(8,128)(2,1)S(1)} %copy-done, f32[1024]{0:T(1024)S(1)} %copy-done.11, f32[1024]{0:T(1024)S(1)} %copy-done.12, f32[512]{0:T(512)S(1)} %add_rsqrt_fusion, f32[512]{0:T(512)S(1)} %broadcast_multiply_fusion, bf16[512,512]{1,0:T(8,128)(2,1)S(1)} %get-tuple-element.37, ...), kind=kOutput, calls=%fused_computation.25 | convolution fusion | flops 1081081856 | bytes 4206592 | tf_op jit(solution)/shard_map/dot_general | solution.py:265
  82.8 0.4 collective-permute-done.22
  83.2 1.3 %collective-permute-done.23 = bf16[32,1024]{1,0:T(8,128)(2,1)S(1)} collective-permute-done((bf16[32,1024]{1,0:T(8,128)(2,1)S(1)}, bf16[32,1024]{1,0:T(8,128)(2,1)S(1)}, u32[]{:S(2)}, u32[]{:S(2)}) %collective-permute-start.23) | collective-permute-done | bytes 65568 | tf_op jit(solution)/shard_map/ppermute | solution.py:115
  84.5 1.0 %convolution_convert_fusion.1 = bf16[128,1024]{1,0:T(8,128)(2,1)} fusion(bf16[128,128]{1,0:T(8,128)(2,1)S(1)} %copy-done.10, bf16[32,1024]{1,0:T(8,128)(2,1)S(1)} %collective-permute-done.25, bf16[32,1024]{1,0:T(8,128)(2,1)S(1)} %collective-permute-done.23, bf16[32,1024]{1,0:T(8,128)(2,1)S(1)} %collective-permute-done.22, ...), kind=kOutput, calls=%fused_computation.26 | convolution fusion | flops 34734080 | bytes 557056 | tf_op jit(solution)/shard_map/dot_general | solution.py:303
  (67 shorter events, 0.6 us)
Async XLA Ops:
  0.6 79.6 %copy-start = (bf16[1024,1024]{1,0:T(8,128)(2,1)S(1)}, bf16[1024,1024]{1,0:T(8,128)(2,1)}, u32[]{:S(2)}) copy-start(bf16[1024,1024]{1,0:T(8,128)(2,1)} %param.18) | copy-start | bytes 6291460
  0.6 12.7 %copy-start.3 = (bf16[31,256]{1,0:T(8,128)(2,1)S(1)}, bf16[31,256]{1,0:T(8,128)(2,1)}, u32[]{:S(2)}) copy-start(bf16[31,256]{1,0:T(8,128)(2,1)} %param.15) | copy-start | bytes 47620
  2.1 9.8 %collective-permute-start = (bf16[256,15]{1,0:T(8,128)(2,1)S(1)}, bf16[256,15]{1,0:T(8,128)(2,1)S(1)}, u32[]{:S(2)}, u32[]{:S(2)}) collective-permute-start(bf16[256,15]{1,0:T(8,128)(2,1)S(1)} %get-tuple-element.60), channel_id=1, source_target_pairs={{0,4},{4,8},{8,12},{12,16},{16,20},{20,24},{24,28},{1,5},{5,9},{9,... | collective-permute-start | bytes 23048 | tf_op jit(solution)/shard_map/ppermute | solution.py:17
  7.0 6.2 %collective-permute-start.1 = (bf16[256,15]{1,0:T(8,128)(2,1)S(1)}, bf16[256,15]{1,0:T(8,128)(2,1)S(1)}, u32[]{:S(2)}, u32[]{:S(2)}) collective-permute-start(bf16[256,15]{1,0:T(8,128)(2,1)S(1)} %get-tuple-element.61), channel_id=1, source_target_pairs={{4,0},{8,4},{12,8},{16,12},{20,16},{24,20},{28,24},{5,1},{9,5},{13... | collective-permute-start | bytes 23048 | tf_op jit(solution)/shard_map/ppermute | solution.py:19
  13.4 14.5 %collective-permute-start.12 = (bf16[32,2048]{1,0:T(8,128)(2,1)}, bf16[32,2048]{1,0:T(8,128)(2,1)S(1)}, u32[]{:S(2)}, u32[]{:S(2)}) collective-permute-start(bf16[32,2048]{1,0:T(8,128)(2,1)} %get-tuple-element.23), channel_id=1, source_target_pairs={{0,4},{4,0},{8,12},{12,8},{16,20},{20,16},{24,28},{28,24},{1,5},{5... | collective-permute-start | bytes 393224 | tf_op jit(solution)/shard_map/ppermute | solution.py:110
  19.5 5.3 %copy-start.9 = (bf16[32,2176]{1,0:T(8,128)(2,1)S(1)}, bf16[32,2176]{1,0:T(8,128)(2,1)}, u32[]{:S(2)}) copy-start(bf16[32,2176]{1,0:T(8,128)(2,1)} %get-tuple-element.24) | copy-start | bytes 417796
  19.5 6.8 %copy-start.8 = (bf16[32,2176]{1,0:T(8,128)(2,1)S(1)}, bf16[32,2176]{1,0:T(8,128)(2,1)}, u32[]{:S(2)}) copy-start(bf16[32,2176]{1,0:T(8,128)(2,1)} %get-tuple-element.25) | copy-start | bytes 417796
  19.5 8.4 %copy-start.7 = (bf16[32,2176]{1,0:T(8,128)(2,1)S(1)}, bf16[32,2176]{1,0:T(8,128)(2,1)}, u32[]{:S(2)}) copy-start(bf16[32,2176]{1,0:T(8,128)(2,1)} %get-tuple-element.26) | copy-start | bytes 417796
  19.5 18.8 %copy-start.4 = (bf16[32,128]{1,0:T(8,128)(2,1)S(1)}, bf16[32,128]{1,0:T(8,128)(2,1)}, u32[]{:S(2)}) copy-start(bf16[32,128]{1,0:T(8,128)(2,1)} %get-tuple-element.27) | copy-start | bytes 24580
  23.0 18.5 %copy-start.2 = (bf16[32,2048]{1,0:T(8,128)(2,1)S(1)}, bf16[32,2048]{1,0:T(8,128)(2,1)}, u32[]{:S(2)}) copy-start(bf16[32,2048]{1,0:T(8,128)(2,1)} %get-tuple-element.23) | copy-start | bytes 393220
  23.1 18.5 %collective-permute-start.2 = (bf16[256,512]{1,0:T(8,128)(2,1)S(1)}, bf16[256,512]{1,0:T(8,128)(2,1)S(1)}, u32[]{:S(2)}, u32[]{:S(2)}) collective-permute-start(bf16[256,512]{1,0:T(8,128)(2,1)S(1)} %pad_maximum_fusion.12), channel_id=1, source_target_pairs={{0,1},{1,0},{2,3},{3,2},{4,5},{5,4},{6,7},{7,6},{8,9},{9,8},{10,11... | collective-permute-start | bytes 786440 | tf_op jit(solution)/shard_map/ppermute | solution.py:110
  23.1 18.5 %collective-permute-start.3 = (bf16[256,512]{1,0:T(8,128)(2,1)S(1)}, bf16[256,512]{1,0:T(8,128)(2,1)S(1)}, u32[]{:S(2)}, u32[]{:S(2)}) collective-permute-start(bf16[256,512]{1,0:T(8,128)(2,1)S(1)} %pad_maximum_fusion.12), channel_id=1, source_target_pairs={{0,2},{1,3},{2,0},{3,1},{4,6},{5,7},{6,4},{7,5},{8,10},{9,11},{10,... | collective-permute-start | bytes 786440 | tf_op jit(solution)/shard_map/ppermute | solution.py:110
  24.7 8.4 %collective-permute-start.5 = (bf16[32,2176]{1,0:T(8,128)(2,1)S(1)}, bf16[32,2176]{1,0:T(8,128)(2,1)S(1)}, u32[]{:S(2)}, u32[]{:S(2)}) collective-permute-start(bf16[32,2176]{1,0:T(8,128)(2,1)S(1)} %copy-done.9), channel_id=1, source_target_pairs={{0,8},{4,12},{8,16},{12,20},{16,24},{20,28},{24,0},{28,4},{1,9},{5... | collective-permute-start | bytes 417800 | tf_op jit(solution)/shard_map/ppermute | solution.py:115
  26.3 12.0 %collective-permute-start.6 = (bf16[32,2176]{1,0:T(8,128)(2,1)S(1)}, bf16[32,2176]{1,0:T(8,128)(2,1)S(1)}, u32[]{:S(2)}, u32[]{:S(2)}) collective-permute-start(bf16[32,2176]{1,0:T(8,128)(2,1)S(1)} %copy-done.8), channel_id=1, source_target_pairs={{0,16},{4,20},{8,24},{12,28},{16,0},{20,4},{24,8},{28,12},{1,17},{... | collective-permute-start | bytes 417800 | tf_op jit(solution)/shard_map/ppermute | solution.py:115
  27.9 10.5 %collective-permute-start.7 = (bf16[32,2176]{1,0:T(8,128)(2,1)S(1)}, bf16[32,2176]{1,0:T(8,128)(2,1)S(1)}, u32[]{:S(2)}, u32[]{:S(2)}) collective-permute-start(bf16[32,2176]{1,0:T(8,128)(2,1)S(1)} %copy-done.7), channel_id=1, source_target_pairs={{0,24},{4,28},{8,0},{12,4},{16,8},{20,12},{24,16},{28,20},{1,25},{... | collective-permute-start | bytes 417800 | tf_op jit(solution)/shard_map/ppermute | solution.py:115
  38.8 6.4 %collective-permute-start.13 = (bf16[32,2048]{1,0:T(8,128)(2,1)S(1)}, bf16[32,2048]{1,0:T(8,128)(2,1)S(1)}, u32[]{:S(2)}, u32[]{:S(2)}) collective-permute-start(bf16[32,2048]{1,0:T(8,128)(2,1)S(1)} %slice.587), channel_id=1, source_target_pairs={{0,4},{4,0},{8,12},{12,8},{16,20},{20,16},{24,28},{28,24},{1,5},{5... | collective-permute-start | bytes 393224 | tf_op jit(solution)/shard_map/ppermute | solution.py:110
  39.3 8.7 %collective-permute-start.14 = (bf16[32,2048]{1,0:T(8,128)(2,1)S(1)}, bf16[32,2048]{1,0:T(8,128)(2,1)S(1)}, u32[]{:S(2)}, u32[]{:S(2)}) collective-permute-start(bf16[32,2048]{1,0:T(8,128)(2,1)S(1)} %slice.588), channel_id=1, source_target_pairs={{0,4},{4,0},{8,12},{12,8},{16,20},{20,16},{24,28},{28,24},{1,5},{5... | collective-permute-start | bytes 393224 | tf_op jit(solution)/shard_map/ppermute | solution.py:110
  41.0 8.8 %collective-permute-start.15 = (bf16[32,2048]{1,0:T(8,128)(2,1)S(1)}, bf16[32,2048]{1,0:T(8,128)(2,1)S(1)}, u32[]{:S(2)}, u32[]{:S(2)}) collective-permute-start(bf16[32,2048]{1,0:T(8,128)(2,1)S(1)} %slice.589), channel_id=1, source_target_pairs={{0,4},{4,0},{8,12},{12,8},{16,20},{20,16},{24,28},{28,24},{1,5},{5... | collective-permute-start | bytes 393224 | tf_op jit(solution)/shard_map/ppermute | solution.py:110
  41.5 9.2 %collective-permute-start.8 = (bf16[128,2048]{1,0:T(8,128)(2,1)S(1)}, bf16[128,2048]{1,0:T(8,128)(2,1)S(1)}, u32[]{:S(2)}, u32[]{:S(2)}) collective-permute-start(bf16[128,2048]{1,0:T(8,128)(2,1)S(1)} %pad_maximum_fusion.9), channel_id=1, source_target_pairs={{0,1},{1,0},{2,3},{3,2},{4,5},{5,4},{6,7},{7,6},{8,9},{9,8},{10,11... | collective-permute-start | bytes 1572872 | tf_op jit(solution)/shard_map/ppermute | solution.py:110
  41.6 8.3 %collective-permute-start.4 = (bf16[256,512]{1,0:T(8,128)(2,1)S(1)}, bf16[256,512]{1,0:T(8,128)(2,1)S(1)}, u32[]{:S(2)}, u32[]{:S(2)}) collective-permute-start(bf16[256,512]{1,0:T(8,128)(2,1)S(1)} %collective-permute-done.3), channel_id=1, source_target_pairs={{0,1},{1,0},{2,3},{3,2},{4,5},{5,4},{6,7},{7,6},{8,9},{9,8},{10,11... | collective-permute-start | bytes 786440 | tf_op jit(solution)/shard_map/ppermute | solution.py:110
  49.8 6.2 %collective-permute-start.16 = (bf16[128,2048]{1,0:T(8,128)(2,1)S(1)}, bf16[128,2048]{1,0:T(8,128)(2,1)S(1)}, u32[]{:S(2)}, u32[]{:S(2)}) collective-permute-start(bf16[128,2048]{1,0:T(8,128)(2,1)S(1)} %constant_dynamic-update-slice_fusion), channel_id=1, source_target_pairs={{0,1},{1,0},{2,3},{3,2},{4,5},{5,4},{6,7},{7,6},{8,9},{9,8},{10,11... | collective-permute-start | bytes 1572872 | tf_op jit(solution)/shard_map/ppermute | solution.py:110
  50.1 2.2 %copy-start.5 = (bf16[1,4096,512]{2,1,0:T(8,128)(2,1)S(1)}, bf16[1,4096,512]{2,1,0:T(8,128)(2,1)}, u32[]{:S(2)}) copy-start(bf16[1,4096,512]{2,1,0:T(8,128)(2,1)} %param.23) | copy-start | bytes 12582916
  52.3 2.2 %copy-start.6 = (bf16[1,4096,512]{2,1,0:T(8,128)(2,1)S(1)}, bf16[1,4096,512]{2,1,0:T(8,128)(2,1)}, u32[]{:S(2)}) copy-start(bf16[1,4096,512]{2,1,0:T(8,128)(2,1)} %param.24) | copy-start | bytes 12582916
  55.3 6.4 %collective-permute-start.10 = (bf16[128,512]{1,0:T(8,128)(2,1)S(1)}, bf16[128,512]{1,0:T(8,128)(2,1)S(1)}, u32[]{:S(2)}, u32[]{:S(2)}) collective-permute-start(bf16[128,512]{1,0:T(8,128)(2,1)S(1)} %multiply_convert_fusion.2), channel_id=1, source_target_pairs={{0,2},{1,3},{2,0},{3,1},{4,6},{5,7},{6,4},{7,5},{8,10},{9,11},{10,... | collective-permute-start | bytes 393224 | tf_op jit(solution)/shard_map/ppermute | solution.py:110
  55.8 5.8 %collective-permute-start.9 = (bf16[128,512]{1,0:T(8,128)(2,1)S(1)}, bf16[128,512]{1,0:T(8,128)(2,1)S(1)}, u32[]{:S(2)}, u32[]{:S(2)}) collective-permute-start(bf16[128,512]{1,0:T(8,128)(2,1)S(1)} %multiply_convert_fusion.2), channel_id=1, source_target_pairs={{0,1},{1,0},{2,3},{3,2},{4,5},{5,4},{6,7},{7,6},{8,9},{9,8},{10,11... | collective-permute-start | bytes 393224 | tf_op jit(solution)/shard_map/ppermute | solution.py:110
  57.6 8.1 %copy-start.1 = (bf16[1,2048,1024]{2,1,0:T(8,128)(2,1)S(1)}, bf16[1,2048,1024]{2,1,0:T(8,128)(2,1)}, u32[]{:S(2)}) copy-start(bf16[1,2048,1024]{2,1,0:T(8,128)(2,1)} %param.25) | copy-start | bytes 12582916
  57.6 6.5 %collective-permute-start.17 = (bf16[128,512]{1,0:T(8,128)(2,1)S(1)}, bf16[128,512]{1,0:T(8,128)(2,1)S(1)}, u32[]{:S(2)}, u32[]{:S(2)}) collective-permute-start(bf16[128,512]{1,0:T(8,128)(2,1)S(1)} %multiply_convert_fusion.1), channel_id=1, source_target_pairs={{0,1},{1,0},{2,3},{3,2},{4,5},{5,4},{6,7},{7,6},{8,9},{9,8},{10,11... | collective-permute-start | bytes 393224 | tf_op jit(solution)/shard_map/ppermute | solution.py:110
  58.0 6.1 %collective-permute-start.18 = (bf16[128,512]{1,0:T(8,128)(2,1)S(1)}, bf16[128,512]{1,0:T(8,128)(2,1)S(1)}, u32[]{:S(2)}, u32[]{:S(2)}) collective-permute-start(bf16[128,512]{1,0:T(8,128)(2,1)S(1)} %multiply_convert_fusion.1), channel_id=1, source_target_pairs={{0,2},{1,3},{2,0},{3,1},{4,6},{5,7},{6,4},{7,5},{8,10},{9,11},{10,... | collective-permute-start | bytes 393224 | tf_op jit(solution)/shard_map/ppermute | solution.py:110
  61.7 2.4 %collective-permute-start.11 = (bf16[128,512]{1,0:T(8,128)(2,1)S(1)}, bf16[128,512]{1,0:T(8,128)(2,1)S(1)}, u32[]{:S(2)}, u32[]{:S(2)}) collective-permute-start(bf16[128,512]{1,0:T(8,128)(2,1)S(1)} %collective-permute-done.10), channel_id=1, source_target_pairs={{0,1},{1,0},{2,3},{3,2},{4,5},{5,4},{6,7},{7,6},{8,9},{9,8},{10,11... | collective-permute-start | bytes 393224 | tf_op jit(solution)/shard_map/ppermute | solution.py:110
  64.0 1.3 %collective-permute-start.19 = (bf16[128,512]{1,0:T(8,128)(2,1)S(1)}, bf16[128,512]{1,0:T(8,128)(2,1)S(1)}, u32[]{:S(2)}, u32[]{:S(2)}) collective-permute-start(bf16[128,512]{1,0:T(8,128)(2,1)S(1)} %collective-permute-done.18), channel_id=1, source_target_pairs={{0,1},{1,0},{2,3},{3,2},{4,5},{5,4},{6,7},{7,6},{8,9},{9,8},{10,11... | collective-permute-start | bytes 393224 | tf_op jit(solution)/shard_map/ppermute | solution.py:110
  66.4 12.1 %collective-permute-start.21 = (bf16[64,1024]{1,0:T(8,128)(2,1)S(1)}, bf16[64,1024]{1,0:T(8,128)(2,1)S(1)}, u32[]{:S(2)}, u32[]{:S(2)}) collective-permute-start(bf16[64,1024]{1,0:T(8,128)(2,1)S(1)} %slice.605), channel_id=1, source_target_pairs={{0,4},{4,0},{8,12},{12,8},{16,20},{20,16},{24,28},{28,24},{1,5},{5... | collective-permute-start | bytes 393224 | tf_op jit(solution)/shard_map/ppermute | solution.py:110
  66.9 7.2 %collective-permute-start.20 = (bf16[32,1024]{1,0:T(8,128)(2,1)S(1)}, bf16[32,1024]{1,0:T(8,128)(2,1)S(1)}, u32[]{:S(2)}, u32[]{:S(2)}) collective-permute-start(bf16[32,1024]{1,0:T(8,128)(2,1)S(1)} %get-tuple-element.50), channel_id=1, source_target_pairs={{0,4},{4,0},{8,12},{12,8},{16,20},{20,16},{24,28},{28,24},{1,5},{5... | collective-permute-start | bytes 196616 | tf_op jit(solution)/shard_map/ppermute | solution.py:110
  68.5 6.3 %collective-permute-start.24 = (bf16[32,1024]{1,0:T(8,128)(2,1)S(1)}, bf16[32,1024]{1,0:T(8,128)(2,1)S(1)}, u32[]{:S(2)}, u32[]{:S(2)}) collective-permute-start(bf16[32,1024]{1,0:T(8,128)(2,1)S(1)} %get-tuple-element.51), channel_id=1, source_target_pairs={{0,4},{4,0},{8,12},{12,8},{16,20},{20,16},{24,28},{28,24},{1,5},{5... | collective-permute-start | bytes 196616 | tf_op jit(solution)/shard_map/ppermute | solution.py:110
  68.9 11.3 %copy-start.11 = (f32[1024]{0:T(1024)S(1)}, f32[1024]{0:T(1024)}, u32[]{:S(2)}) copy-start(f32[1024]{0:T(1024)} %param.17) | copy-start | bytes 12292
  68.9 11.3 %copy-start.12 = (f32[1024]{0:T(1024)S(1)}, f32[1024]{0:T(1024)}, u32[]{:S(2)}) copy-start(f32[1024]{0:T(1024)} %param.16) | copy-start | bytes 12292
  74.9 7.8 %collective-permute-start.25 = (bf16[32,1024]{1,0:T(8,128)(2,1)S(1)}, bf16[32,1024]{1,0:T(8,128)(2,1)S(1)}, u32[]{:S(2)}, u32[]{:S(2)}) collective-permute-start(bf16[32,1024]{1,0:T(8,128)(2,1)S(1)} %get-tuple-element.49), channel_id=1, source_target_pairs={{0,8},{4,12},{8,16},{12,20},{16,24},{20,28},{24,0},{28,4},{1,9},{5... | collective-permute-start | bytes 196616 | tf_op jit(solution)/shard_map/ppermute | solution.py:115
  78.7 4.5 %collective-permute-start.22 = (bf16[32,1024]{1,0:T(8,128)(2,1)S(1)}, bf16[32,1024]{1,0:T(8,128)(2,1)S(1)}, u32[]{:S(2)}, u32[]{:S(2)}) collective-permute-start(bf16[32,1024]{1,0:T(8,128)(2,1)S(1)} %get-tuple-element.62), channel_id=1, source_target_pairs={{0,24},{4,28},{8,0},{12,4},{16,8},{20,12},{24,16},{28,20},{1,25},{... | collective-permute-start | bytes 196616 | tf_op jit(solution)/shard_map/ppermute | solution.py:115
  79.2 5.3 %copy-start.10 = (bf16[128,128]{1,0:T(8,128)(2,1)S(1)}, bf16[128,128]{1,0:T(8,128)(2,1)}, u32[]{:S(2)}) copy-start(bf16[128,128]{1,0:T(8,128)(2,1)} %get-tuple-element.22) | copy-start | bytes 98308
  79.2 5.3 %collective-permute-start.23 = (bf16[32,1024]{1,0:T(8,128)(2,1)S(1)}, bf16[32,1024]{1,0:T(8,128)(2,1)S(1)}, u32[]{:S(2)}, u32[]{:S(2)}) collective-permute-start(bf16[32,1024]{1,0:T(8,128)(2,1)S(1)} %get-tuple-element.63), channel_id=1, source_target_pairs={{0,16},{4,20},{8,24},{12,28},{16,0},{20,4},{24,8},{28,12},{1,17},{... | collective-permute-start | bytes 196616 | tf_op jit(solution)/shard_map/ppermute | solution.py:115
